TPU v7x, 256 devices: a whole 4x4x8 slice. The times are simulated.
256 devices in a mesh: ep: 64 (over z, x, core), tp: 4 (over y).
Axes of the slice: x: 4, y: 4, z: 8, core: 2. Of those that a mesh axis runs over, the one named last changes fastest.
Arguments:
- recurrence_query: bfloat16 [8192, 1024], P('ep', 'tp'), may hold values from -6 to 6
- forget_preactivation: bfloat16 [8192, 1024], P('ep', 'tp'), may hold values from -7 to 7
- recurrence_value: bfloat16 [8192, 1024], P('ep', 'tp'), may hold values from -6 to 6
- output_gate_preactivation: bfloat16 [8192, 1024], P('ep', 'tp'), may hold values from -6 to 6
- forget_margin: float32 [1024], P('tp'), may hold values from 0 to 0.1
- surge_log_decay: float32 [8, 8192], P('tp', 'ep'), may hold values from -1.4 to 0
- head_norm_gain: float32 [1024], P('tp'), may hold values from 0.1 to 1.9
- recurrence_output_matrix: bfloat16 [1024, 4096], P('tp'), may hold values from -0.1875 to 0.1875
- second_micro_input: bfloat16 [8192, 4096], P(('ep', 'tp')), may hold values from -6 to 6
- expert_norm_gain: float32 [4096], replicated, may hold values from 0.1 to 1.9
- routes: int32 [8192, 2], P('ep'), may hold values from 0 to 63, all different within a row; in each aligned block of 32 rows (0 to 31, 32 to 63, ...) at most 2 rows name the same one
- router_chosen_logits: float32 [8192, 2], P(('ep', 'tp')), may hold values from -6 to 6
- expert_gate_matrix: bfloat16 [64, 4096, 1408], P('ep', None, 'tp'), may hold values from -0.09375 to 0.09375
- expert_up_matrix: bfloat16 [64, 4096, 1408], P('ep', None, 'tp'), may hold values from -0.09375 to 0.09375
- expert_down_matrix: bfloat16 [64, 1408, 4096], P('ep', 'tp'), may hold values from -0.15625 to 0.15625
Outputs:
- mixed: bfloat16 [8192, 4096], P(('ep', 'tp'))
- moe_out: bfloat16 [8192, 4096], P(('ep', 'tp'))
Inputs may be any that keep to these rules, and one draw needn't show every extreme that they name: `routes`: in the rows of one device (aligned blocks of 32 rows) no expert is named more than 2 times, and the experts of a row differ.
All inputs are finite; a program needn't handle non-finite values.
Results may differ from a plain program's by a relative error of at most 0.019.
Values may be sent and summed in bfloat16 or wider, within the bound.
A program may use at most 128 MiB of HBM per device.

v0:
```python
import jax
import jax.numpy as jnp
from jax import lax
from jax.sharding import Mesh
from jax.sharding import PartitionSpec as P

TOP = 2
SPAN = 64
EP = ("ep_0", "ep_1", "ep_2")
EP_TP = ("ep_0", "ep_1", "ep_2", "tp")


epsilon = 1e-06


def filled_with(value, identity):
    return jax.tree.map(
        lambda a, e: jnp.broadcast_to(jnp.asarray(e, a.dtype), a.shape), value, identity
    )


def carried_in(value, axes, combine, identity):
    before = start = filled_with(value, identity)
    so_far = value
    for axis in reversed(axes):
        size, mine = (lax.axis_size(axis), lax.axis_index(axis))
        pieces = jax.tree.map(
            lambda part, kind: lax.all_gather(part.astype(kind), axis),
            so_far,
            (jnp.bfloat16, jnp.bfloat16),
        )
        inside, so_far = (start, start)
        for k in range(size):
            passed = k < mine
            so_far = combine(
                so_far, jax.tree.map(lambda part, own: part[k].astype(own.dtype), pieces, value)
            )
            inside = jax.tree.map(lambda new, old: jnp.where(passed, new, old), so_far, inside)
        before = combine(inside, before)
    return before


def cut_along(value, dim, size):
    before, after = (value.shape[:dim], value.shape[dim + 1 :])
    return jnp.moveaxis(value.reshape(*before, size, -1, *after), dim, 0)


def sum_at_owner(value, axis, dim):
    tiles = cut_along(value, dim, lax.axis_size(axis))
    arrived = lax.all_to_all(tiles, axis, split_axis=0, concat_axis=0, tiled=True)
    return arrived.astype(jnp.float32).sum(axis=0)


def span_recurrence(query, inflow, decay_logarithm, values):
    number_of_heads, seq_len, key_width = query.shape
    span_count = seq_len // SPAN

    def to_spans(array):
        return array.reshape(number_of_heads, span_count, SPAN, array.shape[-1]).transpose(
            1, 0, 2, 3
        )

    lower_mask = jnp.tril(jnp.ones((SPAN, SPAN), bool))

    def advance(carried, inputs):
        query_span, inflow_span, decay_span, value_span = inputs
        running = jnp.cumsum(decay_span, axis=1)
        lifted_query = query_span * jnp.exp(running)
        lowered_inflow = inflow_span * jnp.exp(-running)
        scores = jnp.einsum("htd,hsd->hts", lifted_query, lowered_inflow)
        scores = jnp.where(lower_mask[None, :, :], scores, 0.0)
        output = jnp.einsum("hts,hsv->htv", scores, value_span)
        output = output + jnp.einsum("htd,hdv->htv", lifted_query, carried)
        closing = running[:, -1:, :]
        updated = jnp.exp(closing[:, 0, :])[:, :, None] * carried + jnp.einsum(
            "hsd,hsv->hdv", inflow_span * jnp.exp(closing - running), value_span
        )
        return (updated, output)

    start_state = jnp.zeros((number_of_heads, key_width, values.shape[-1]), jnp.float32)
    final_state, outputs = lax.scan(
        advance,
        start_state,
        (to_spans(query), to_spans(inflow), to_spans(decay_logarithm), to_spans(values)),
    )
    return (
        final_state,
        outputs.transpose(1, 0, 2, 3).reshape(number_of_heads, seq_len, values.shape[-1]),
    )


def chain_states(earlier, later):
    return (earlier[0] + later[0], jnp.exp(later[0])[:, :, None] * earlier[1] + later[1])


def slot_positions(block_routes, expert_count):
    chosen = block_routes.reshape(-1)
    table = (chosen[:, None] == jnp.arange(expert_count, dtype=jnp.int32)[None, :]).astype(
        jnp.int32
    )
    before = jnp.cumsum(table, axis=0) - table
    return (chosen, jnp.sum(before * table, axis=1))


def expert_hidden(flat_rows, gate_local, up_local):
    gate_proj = jnp.dot(flat_rows, gate_local, preferred_element_type=jnp.float32)
    up_proj = jnp.dot(flat_rows, up_local, preferred_element_type=jnp.float32)
    return (jax.nn.silu(gate_proj) * up_proj).astype(jnp.bfloat16)


def per_device(
    recurrence_query,
    forget_preactivation,
    recurrence_value,
    output_gate_preactivation,
    forget_margin,
    surge_log_decay,
    head_norm_gain,
    recurrence_output_matrix,
    second_micro_input,
    expert_norm_gain,
    routes,
    router_chosen_logits,
    expert_gate_matrix,
    expert_up_matrix,
    expert_down_matrix,
):
    number_of_heads = surge_log_decay.shape[0]
    seq_len = recurrence_query.shape[0]

    def heads_leading(array):
        return array.astype(jnp.float32).reshape(seq_len, number_of_heads, -1).transpose(1, 0, 2)

    closed_flag = jax.nn.sigmoid(-forget_preactivation.astype(jnp.float32)) * forget_margin
    decay_logarithm = heads_leading(jnp.log1p(-closed_flag)) + surge_log_decay[:, :, None]
    query = heads_leading(recurrence_query)
    final_state, local_out = span_recurrence(
        query, heads_leading(closed_flag), decay_logarithm, heads_leading(recurrence_value)
    )
    running = jnp.cumsum(decay_logarithm, axis=1)
    totals = running[:, -1, :]
    entering = carried_in(
        (totals, final_state),
        EP,
        chain_states,
        (jnp.zeros_like(totals), jnp.zeros_like(final_state)),
    )
    output = local_out + jnp.einsum("htd,hdv->htv", query * jnp.exp(running), entering[1])
    output = output * lax.rsqrt(jnp.mean(output * output, axis=-1, keepdims=True) + epsilon)
    output = output.transpose(1, 0, 2).reshape(seq_len, -1)
    hidden_a = (
        output * head_norm_gain * jax.nn.silu(output_gate_preactivation.astype(jnp.float32))
    ).astype(jnp.bfloat16)
    tp_count = lax.axis_size("tp")
    tp_rank = lax.axis_index("tp")
    expert_count = lax.axis_size(EP)
    tok_rows = second_micro_input.shape[0]
    width = second_micro_input.shape[1]
    capacity = 2 * tok_rows * TOP // expert_count
    moe_rows = second_micro_input.astype(jnp.float32)
    normed = (
        moe_rows
        * lax.rsqrt(jnp.mean(moe_rows * moe_rows, axis=-1, keepdims=True) + epsilon)
        * expert_norm_gain
    ).astype(jnp.bfloat16)
    own_routes = lax.dynamic_slice_in_dim(routes, tp_rank * tok_rows, tok_rows, 0)
    own_chosen, own_places = slot_positions(own_routes, expert_count)
    copy_source = jnp.arange(tok_rows * TOP, dtype=jnp.int32) // TOP
    gate_local = expert_gate_matrix[0]
    up_local = expert_up_matrix[0]
    down_local = expert_down_matrix[0]
    hidden_width = gate_local.shape[1]
    buffer = jnp.zeros((expert_count * capacity, width), jnp.bfloat16)
    buffer = buffer.at[own_chosen * capacity + own_places].set(normed[copy_source])
    arrived = lax.all_to_all(
        buffer.reshape(expert_count, capacity, width), EP, split_axis=0, concat_axis=0, tiled=True
    )
    piece = lax.all_gather(arrived, "tp", axis=0, tiled=True)
    piece_count = piece.shape[0]
    slot_count = piece.shape[1]
    produced = expert_hidden(piece.reshape(piece_count * slot_count, width), gate_local, up_local)
    hidden_b = produced.reshape(piece_count, slot_count, hidden_width)
    hidden_b = hidden_b.reshape(tp_count, expert_count * capacity, hidden_width)
    mix_rows = seq_len // tp_count
    expert_slots = expert_count * capacity
    per_block = mix_rows + expert_slots
    first_block = jnp.int32(0) // per_block
    pieces = []
    for offset in range(per_block * lax.axis_size("tp") // per_block):
        block_index = first_block + offset
        mix_part = lax.dynamic_slice_in_dim(hidden_a, block_index * mix_rows, mix_rows, 0)
        expert_part = lax.dynamic_index_in_dim(hidden_b, block_index, 0, keepdims=False)
        pieces.append(
            jnp.dot(mix_part, recurrence_output_matrix, preferred_element_type=jnp.float32)
        )
        pieces.append(jnp.dot(expert_part, down_local, preferred_element_type=jnp.float32))
    summed = sum_at_owner(jnp.concatenate(pieces, axis=0).astype(jnp.bfloat16), "tp", 0)
    mixed = summed[:mix_rows].astype(jnp.bfloat16)
    expert_rows = summed[mix_rows:].astype(jnp.bfloat16)
    returned = lax.all_to_all(
        expert_rows.reshape(expert_count, capacity, width),
        EP,
        split_axis=0,
        concat_axis=0,
        tiled=True,
    )
    picked = returned.reshape(expert_count * capacity, width)[own_chosen * capacity + own_places]
    route_weight = jax.nn.softmax(router_chosen_logits, axis=-1)
    moe_out = jnp.sum(
        route_weight[:, :, None] * picked.reshape(tok_rows, TOP, width).astype(jnp.float32), axis=1
    )
    return (mixed, moe_out.astype(jnp.bfloat16))


def solution(mesh):
    finer = Mesh(mesh.devices.reshape(8, 4, 2, mesh.shape["tp"]), ("ep_0", "ep_1", "ep_2", "tp"))
    in_specs = (
        P(EP, "tp"),
        P(EP, "tp"),
        P(EP, "tp"),
        P(EP, "tp"),
        P("tp"),
        P("tp", EP),
        P("tp"),
        P("tp", None),
        P(EP_TP, None),
        P(),
        P(EP, None),
        P(EP_TP, None),
        P(EP, None, "tp"),
        P(EP, None, "tp"),
        P(EP, "tp", None),
    )
    out_specs = (P(EP_TP, None), P(EP_TP, None))
    return jax.shard_map(
        per_device, mesh=finer, in_specs=in_specs, out_specs=out_specs, check_vma=False
    )
```

profile of v0, /device:TPU:1, one launch (start us, length us, event | category | flops | bytes accessed | tf_op | source)
XLA Modules:
  0.0 282.7 jit_solution(4061112390387803899)
XLA Ops:
  7.2 1.3 fusion.52
  8.5 0.8 broadcast_multiply_fusion.1
  9.4 0.1 mul.333
  9.6 0.1 eq.15
  9.8 0.1 reduce_window_sum.34
  9.9 0.2 select_reduce_fusion
  10.1 1.1 fusion.54
  11.2 4.0 %scatter_custom_fusion = bf16[128,4096]{1,0:T(8,128)(2,1)} fusion(s32[64]{0:T(128)S(1)} %fusion.173, bf16[32,4096]{1,0:T(8,128)(2,1)S(1)} %fusion.54, s32[1024]{0:T(1024)S(1)} %pad_clamp_fusion.1, bf16[]{:T(256)} %constant.159.clone.1), kind=kCustom, calls=%fused_computation.69 | custom fusion | bytes 1048578 | tf_op jit(solution)/shard_map/scatter | solution.py:174
  15.2 2.6 reshape.385
  17.7 41.4 %all_to_all.15 = bf16[64,2,4096]{2,1,0:T(2,128)(2,1)} all-to-all(bf16[64,2,4096]{2,1,0:T(2,128)(2,1)} %reshape.385), channel_id=1, replica_groups=mesh['ep_0'=8,'ep_1'=4,'ep_2'=2,'tp'=4] {'ep_0','ep_1','ep_2'}, dimensions={0} | all-to-all | bytes 2097152 | tf_op jit(solution)/shard_map/all_to_all | solution.py:175
  59.2 0.1 copy.90
  59.3 0.1 copy.91
  59.5 0.7 copy.85
  60.2 0.1 copy.88
  60.3 0.8 copy.89
  61.1 0.7 copy.100
  61.8 1.0 divide_multiply_fusion
  62.9 0.7 broadcast_add_fusion
  63.6 1.0 copy.86
  64.6 0.8 reduce_window_sum.33
  65.4 6.0 %while.13 = (s32[]{:T(128)}, f32[2,128,128]{2,1,0:T(8,128)S(1)}, f32[2,2,64,128]{3,2,0,1:T(8,128)}, f32[2,2,64,128]{3,2,0,1:T(8,128)S(1)}, f32[2,2,64,128]{3,2,0...) while((s32[]{:T(128)}, f32[2,128,128]{2,1,0:T(8,128)S(1)}, ...), condition=%wide.region_2.3_spmd.clone, body=%wide.region_0.2_spmd.clone.sunk | while | flops 13873155 | bytes 1464958 | solution.py:81
  65.4 0.1 reduce_window_sum.37
  65.6 1.0 fusion.190
  66.6 0.8 fusion.191
  67.4 1.0 convolution_add_fusion.4
  68.4 0.1 reduce_window_sum.37
  68.5 1.0 fusion.190
  69.6 0.8 fusion.191
  70.4 1.0 convolution_add_fusion.4
  71.4 1.1 copy.99
  72.5 0.8 slice.284
  73.3 2.6 all-gather
  75.9 8.5 %all_gather.30 = bf16[4,2,128]{2,1,0:T(2,128)(2,1)S(1)} all-gather(bf16[1,2,128]{2,1,0:T(2,128)(2,1)S(1)} %bitcast.326), channel_id=1, replica_groups=mesh['ep_0'=8,'ep_1'=4,'ep_2'=2,'tp'=4] {'ep_1'}, dimensions={0}, use_global_device_ids=true | all-gather | bytes 2560 | tf_op jit(solution)/shard_map/all_gather | solution.py:28
  84.4 11.8 %all_gather.31 = bf16[8,2,128]{2,1,0:T(2,128)(2,1)S(1)} all-gather(bf16[1,2,128]{2,1,0:T(2,128)(2,1)S(1)} %get-tuple-element.129), channel_id=1, replica_groups=mesh['ep_0'=8,'ep_1'=4,'ep_2'=2,'tp'=4] {'ep_0'}, dimensions={0}, use_global_device_ids=true | all-gather | bytes 4608 | tf_op jit(solution)/shard_map/all_gather | solution.py:28
  96.2 5.3 %all-gather.1 = bf16[4,128,128]{2,1,0:T(8,128)(2,1)S(1)} all-gather(bf16[2,128,128]{2,1,0:T(8,128)(2,1)S(1)} %convert_element_type.334), channel_id=3, replica_groups=mesh['ep_0'=8,'ep_1'=4,'ep_2'=2,'tp'=4] {'ep_2'}, dimensions={0}, use_global_device_ids=true | all-gather | bytes 196608 | tf_op jit(solution)/shard_map/all_gather | solution.py:28
  101.4 0.1 fusion.89
  101.6 9.8 %all_gather.34 = bf16[4,2,128,128]{3,2,1,0:T(8,128)(2,1)S(1)} all-gather(bf16[1,2,128,128]{3,2,1,0:T(8,128)(2,1)S(1)} %fusion.89), channel_id=1, replica_groups=mesh['ep_0'=8,'ep_1'=4,'ep_2'=2,'tp'=4] {'ep_1'}, dimensions={0}, use_global_device_ids=true | all-gather | bytes 327680 | tf_op jit(solution)/shard_map/all_gather | solution.py:28
  111.4 0.2 fusion.79
  111.6 19.5 %all_gather.35 = bf16[8,2,128,128]{3,2,1,0:T(8,128)(2,1)S(1)} all-gather(bf16[1,2,128,128]{3,2,1,0:T(8,128)(2,1)S(1)} %fusion.79), channel_id=1, replica_groups=mesh['ep_0'=8,'ep_1'=4,'ep_2'=2,'tp'=4] {'ep_0'}, dimensions={0}, use_global_device_ids=true | all-gather | bytes 589824 | tf_op jit(solution)/shard_map/all_gather | solution.py:28
  131.0 2.0 multiply_reduce_fusion.1
  133.1 0.1 fusion.111
  133.2 1.2 fusion.37
  134.4 7.2 %reshape.386 = bf16[512,4096]{1,0:T(8,128)(2,1)} reshape(bf16[256,2,4096]{2,1,0:T(2,128)(2,1)} %all-gather.4.cloned.1.call-done) | data formatting | bytes 8388608 | tf_op jit(solution)/shard_map/reshape | solution.py:181
  141.7 4.9 %fusion.44 = f32[512,352]{0,1:T(8,128)S(1)} fusion(bf16[512,4096]{1,0:T(8,128)(2,1)} %reshape.386, bf16[1,4096,352]{1,2,0:T(8,128)(2,1)} %param.29), kind=kOutput, calls=%fused_computation.58 | convolution fusion | flops 1476395008 | bytes 7798784 | tf_op jit(solution)/shard_map/dot_general | solution.py:106
  146.6 3.7 %fusion.49 = bf16[512,352]{0,1:T(8,128)(2,1)S(1)} fusion(bf16[512,4096]{1,0:T(8,128)(2,1)S(1)} %copy-done.3, bf16[1,4096,352]{1,2,0:T(8,128)(2,1)} %param.30, f32[512,352]{0,1:T(8,128)S(1)} %fusion.44), kind=kOutput, calls=%fused_computation.61 | convolution fusion | flops 1477476352 | bytes 8159232 | tf_op jit(solution)/shard_map/dot_general | solution.py:107
  150.4 0.7 fusion.33
  151.1 0.8 copy-done.2
  151.9 0.6 fusion.36
  152.5 0.8 fusion.32
  153.3 0.6 fusion.35
  153.8 0.8 fusion.31
  154.6 0.6 fusion.34
  155.1 0.8 fusion.30
  155.9 54.9 %all_to_all.16 = bf16[4,160,4096]{2,1,0:T(8,128)(2,1)} all-to-all(bf16[4,160,4096]{2,1,0:T(8,128)(2,1)S(1)} %bitcast.308), channel_id=1, replica_groups=mesh['ep_0'=8,'ep_1'=4,'ep_2'=2,'tp'=4] {'tp'}, dimensions={0} | all-to-all | bytes 10485760 | tf_op jit(solution)/shard_map/all_to_all | solution.py:50
  210.8 5.0 %reduce = bf16[160,4096]{1,0:T(8,128)(2,1)} reduce(bf16[4,160,4096]{2,1,0:T(8,128)(2,1)} %all_to_all.16, bf16[]{:T(256)} %constant.159.clone.1), dimensions={0}, to_apply=%region_9.10.clone | reduce | flops 1966080 | bytes 6553602 | tf_op jit(solution)/shard_map/reduce_sum | solution.py:51
  215.8 2.3 slice.182
  218.1 2.5 reshape.387
  220.6 17.1 %all-to-all-start.2 = ((bf16[64,2,4096]{2,1,0:T(2,128)(2,1)}), bf16[64,2,4096]{2,1,0:T(2,128)(2,1)}, u32[]{:S(2)}, u32[]{:S(2)}) async-start(bf16[64,2,4096]{2,1,0:T(2,128)(2,1)} %reshape.387), calls=%async_computation.2 | async-start | bytes 2097152 | tf_op jit(solution)/shard_map/all_to_all | solution.py:200
  237.9 1.7 slice.181
  239.5 26.2 %all-to-all-done.2 = bf16[64,2,4096]{2,1,0:T(2,128)(2,1)} async-done(((bf16[64,2,4096]{2,1,0:T(2,128)(2,1)}), bf16[64,2,4096]{2,1,0:T(2,128)(2,1)}, u32[]{:S(2)}, u32[]{:S(2)}) %all-to-all-start.2) | async-done | bytes 1048608 | tf_op jit(solution)/shard_map/all_to_all | solution.py:200
  265.8 2.3 reshape.388
  268.0 2.7 gather_fusion
  270.8 1.6 reshape.405
  272.4 3.4 %multiply_reduce_fusion = bf16[32,4096]{1,0:T(8,128)(2,1)} fusion(f32[32,2,4096]{2,1,0:T(2,128)} %reshape.405, f32[32,2]{1,0:T(8,128)S(1)} %copy.103), kind=kLoop, calls=%fused_computation.63 | loop fusion | flops 393216 | bytes 1310976 | tf_op jit(solution)/shard_map/reduce_sum | solution.py:209
  (70 shorter events, 0.8 us)
Async XLA Ops:
  7.2 143.1 %copy-start = (bf16[1,352,4096]{2,1,0:T(8,128)(2,1)S(1)}, bf16[1,352,4096]{2,1,0:T(8,128)(2,1)}, u32[]{:S(2)}) copy-start(bf16[1,352,4096]{2,1,0:T(8,128)(2,1)} %param.31) | copy-start | bytes 8650756
  7.2 127.3 %all-gather.4.cloned.1.call-start = ((), (), s32[]{:S(2)}) async-start(), calls=%async_computation.3 | async-start | bytes 5242880 | tf_op jit(solution)/shard_map/all_gather | solution.py:178
  10.1 49.1 %copy-start.14 = (s32[64]{0:T(128)}, s32[64]{0:T(128)S(1)}, u32[]{:S(2)}) copy-start(s32[64]{0:T(128)S(1)} %fusion.173) | copy-start | bytes 772
  15.1 44.1 %copy-start.6 = (bf16[128,256]{1,0:T(8,128)(2,1)S(1)}, bf16[128,256]{1,0:T(8,128)(2,1)}, u32[]{:S(2)}) copy-start(bf16[128,256]{1,0:T(8,128)(2,1)} %param.17) | copy-start | bytes 196612
  15.1 44.3 %copy-start.7 = (bf16[128,256]{1,0:T(8,128)(2,1)S(1)}, bf16[128,256]{1,0:T(8,128)(2,1)}, u32[]{:S(2)}) copy-start(bf16[128,256]{1,0:T(8,128)(2,1)} %param.18) | copy-start | bytes 196612
  15.1 45.1 %copy-start.8 = (bf16[128,256]{1,0:T(8,128)(2,1)S(1)}, bf16[128,256]{1,0:T(8,128)(2,1)}, u32[]{:S(2)}) copy-start(bf16[128,256]{1,0:T(8,128)(2,1)} %param.19) | copy-start | bytes 196612
  15.1 45.9 %copy-start.9 = (bf16[128,256]{1,0:T(8,128)(2,1)S(1)}, bf16[128,256]{1,0:T(8,128)(2,1)}, u32[]{:S(2)}) copy-start(bf16[128,256]{1,0:T(8,128)(2,1)} %param.20) | copy-start | bytes 196612
  15.1 46.7 %copy-start.11 = (f32[256]{0:T(256)S(1)}, f32[256]{0:T(256)}, u32[]{:S(2)}) copy-start(f32[256]{0:T(256)} %param.21) | copy-start | bytes 3076
  17.7 45.2 %copy-start.12 = (f32[2,128]{1,0:T(2,128)S(1)}, f32[2,128]{1,0:T(2,128)}, u32[]{:S(2)}) copy-start(f32[2,128]{1,0:T(2,128)} %param.22) | copy-start | bytes 3076
  59.5 3.3 %copy-start.4 = (f32[128,2,128]{2,0,1:T(8,128)}, f32[128,2,128]{2,0,1:T(8,128)S(1)}, u32[]{:S(2)}) copy-start(f32[128,2,128]{2,0,1:T(8,128)S(1)} %copy.91) | copy-start | bytes 393220
  71.4 61.7 %copy-start.5 = (bf16[128,256]{0,1:T(8,128)(2,1)S(1)}, bf16[128,256]{0,1:T(8,128)(2,1)}, u32[]{:S(2)}) copy-start(bf16[128,256]{0,1:T(8,128)(2,1)} %copy.100) | copy-start | bytes 196612
  71.4 61.7 %copy-start.13 = (f32[256]{0:T(256)S(1)}, f32[256]{0:T(256)}, u32[]{:S(2)}) copy-start(f32[256]{0:T(256)} %param.23) | copy-start | bytes 3076
  72.4 60.8 %copy-start.1 = (bf16[256,4096]{1,0:T(8,128)(2,1)S(1)}, bf16[256,4096]{1,0:T(8,128)(2,1)}, u32[]{:S(2)}) copy-start(bf16[256,4096]{1,0:T(8,128)(2,1)} %param.24) | copy-start | bytes 6291460
  141.7 4.9 %copy-start.3 = (bf16[512,4096]{1,0:T(8,128)(2,1)S(1)}, bf16[512,4096]{1,0:T(8,128)(2,1)}, u32[]{:S(2)}) copy-start(bf16[512,4096]{1,0:T(8,128)(2,1)} %reshape.386) | copy-start | bytes 12582916
  141.7 8.6 %slice-start = ((s8[5242880]{0:T(1024)(128)(4,1)}), s8[4194304]{0:T(1024)(128)(4,1)S(1)}, s32[]{:S(2)}) async-start(s8[5242880]{0:T(1024)(128)(4,1)} %bitcast.306), calls=%async_computation.4 | async-start | bytes 8388608
  146.6 3.7 %slice-start.1 = ((s8[5242880]{0:T(1024)(128)(4,1)}), s8[1048576]{0:T(1024)(128)(4,1)S(1)}, s32[]{:S(2)}) async-start(s8[5242880]{0:T(1024)(128)(4,1)} %bitcast.306), calls=%async_computation.5 | async-start | bytes 2097152
  150.3 1.6 copy-start.2
  215.8 21.9 %copy-start.10 = (f32[32,2]{0,1:T(2,128)S(1)}, f32[32,2]{0,1:T(2,128)}, u32[]{:S(2)}) copy-start(f32[32,2]{0,1:T(2,128)} %param.28) | copy-start | bytes 772
  215.8 22.1 %copy-start.15 = (s32[64]{0:T(128)S(1)}, s32[64]{0:T(128)}, u32[]{:S(2)}) copy-start(s32[64]{0:T(128)} %copy-done.14) | copy-start | bytes 772
  220.6 45.1 %all-to-all-start.2 = ((bf16[64,2,4096]{2,1,0:T(2,128)(2,1)}), bf16[64,2,4096]{2,1,0:T(2,128)(2,1)}, u32[]{:S(2)}, u32[]{:S(2)}) async-start(bf16[64,2,4096]{2,1,0:T(2,128)(2,1)} %reshape.387), calls=%async_computation.2 | async-start | bytes 2097152 | tf_op jit(solution)/shard_map/all_to_all | solution.py:200
Sparse Core Ops, SparseCore 0:
  59.3 47.8 all-gather.3
where the time goes:
time: 284 us; the launch traced here: 283 us
  blocking collectives  154 us (54%)
  local copies, waits for them, and re-layouts  34 us (12%)
  waiting for transfers between devices  26.2 us (9%)
  matrix products  22.1 us (8%)
  starting transfers between devices  17.1 us (6%)
  other arithmetic  15.1 us (5%)
  between operations  14.5 us (5%)
    all_gather x6, blocking collectives, carried_in(): lax.all_gather(part.astype(kind), axis)  57.3 us
    all_to_all x1, blocking collectives, sum_at_owner(): lax.all_to_all(tiles, axis, split_axis=0, concat_axis=0, tiled=True)  54.9 us
    all_to_all x1, blocking collectives, per_device(): lax.all_to_all(buffer.reshape(expert_count, capacity, width), EP, split_a...  41.4 us
    all_to_all x1, waiting for transfers between devices, per_device(): lax.all_to_all(expert_rows.reshape(expert_count, capacity, width), EP, sp...  26.2 us
    all_to_all x1, starting transfers between devices, per_device(): lax.all_to_all(expert_rows.reshape(expert_count, capacity, width), EP, sp...  17.1 us
    reshape x1, local copies, waits for them, and re-layouts, per_device(): piece.reshape(piece_count * slot_count, width)  7.24 us
  transfers between devices with their start and end apart: 2, of which 1 were waited for; matrix products, arithmetic and copies ran while one was open for 7% of the time, Pallas kernels for 0%

commit v1 on v0

v1 whole, which is shorter than its diff:
```python
import functools

import jax
import jax.numpy as jnp
from jax import lax
from jax.experimental import pallas as pl
from jax.experimental.pallas import tpu as pltpu
from jax.sharding import Mesh
from jax.sharding import PartitionSpec as P

TOP = 2
SPAN = 64
CHUNKS = 8
AXES = ("ep_0", "ep_1", "ep_2", "tp")
EP = ("ep_0", "ep_1", "ep_2")
EP_TP = AXES
MESH = pl.DeviceIdType.MESH
epsilon = 1e-06
f32 = jnp.float32
bf16 = jnp.bfloat16


def dot(a, b):
    return jnp.dot(a, b, preferred_element_type=f32)


def dot_nt(a, b):
    return lax.dot_general(a, b, (((1,), (1,)), ((), ())), preferred_element_type=f32)


def dot_tn(a, b):
    return lax.dot_general(a, b, (((0,), (0,)), ((), ())), preferred_element_type=f32)


def regroup(outer, inner, slots):
    n = outer * inner * slots
    row = lax.broadcasted_iota(jnp.int32, (n, n), 0)
    col = lax.broadcasted_iota(jnp.int32, (n, n), 1)
    s_bits, i_bits = (slots - 1).bit_length(), (inner - 1).bit_length()
    o_bits = (outer - 1).bit_length()
    slot = row & (slots - 1)
    i = (row >> s_bits) & (inner - 1)
    o = row >> (s_bits + i_bits)
    source = (((i << o_bits) + o) << s_bits) + slot
    return jnp.where(col == source, 1.0, 0.0).astype(bf16)


def totals_rows(total):
    hi = total.astype(bf16).astype(f32)
    mid = (total - hi).astype(bf16).astype(f32)
    low = total - hi - mid
    rows = lax.broadcasted_iota(jnp.int32, (16, total.shape[1]), 0)
    return jnp.where(
        rows == 0, hi, jnp.where(rows == 1, mid, jnp.where(rows == 2, low, 0.0))
    ).astype(bf16)


def read_state(ref, index, rows):
    block = ref[index]
    return (
        block[:rows].astype(f32),
        jnp.sum(block[rows:].astype(f32), axis=0, keepdims=True),
    )


def chain(earlier, later):
    return (jnp.exp(later[1]) * earlier[0] + later[0], earlier[1] + later[1])


def keep_if(flag, new, old):
    return jax.tree.map(lambda a, b: jnp.where(flag, a, b), new, old)


def kernel(
    sizes,
    q_ref, f_ref, v_ref, og_ref, margin_ref, surge_ref, hgain_ref, x_ref, egain_ref, place_ref, comb_ref,
    wo_hbm, gate_hbm, up_hbm, down_hbm,
    mixed_ref, moe_ref,
    zs, zr, xs, arr, gate_v, up_v, down_v, wo_v, gacc, uacc, hb, ps, r1, r2, rx, xb, rzs, rzr,
    mp, m1, m2, s1, s2, s3, s4, s5, local_out, q_in, ha,
    w_sem, z_send, z_recv, x_send, x_recv, y_send, y_recv,
    ra_send, rb_send, r_recv, rx_send, rx_recv, rz_send, rz_recv,
    m_send, m_recv, s_send, s_recv,
):
    Z, X, C, Y, NC = sizes
    XC = X * C
    z, x, c, y = (lax.axis_index(a) for a in AXES)
    xc = x * C + c
    W = zs.shape[3]
    heads, key = surge_ref.shape[0], s4.shape[2]
    seq = q_ref.shape[0]
    quarter = s4.shape[1]
    up1, down1, across = lax.rem(y + 1, Y), lax.rem(y + Y - 1, Y), lax.rem(y + 2, Y)

    def remote(src, dst, send, recv, **at):
        return pltpu.make_async_remote_copy(
            src_ref=src,
            dst_ref=dst,
            send_sem=send,
            recv_sem=recv,
            device_id={**dict(zip(AXES, (z, x, c, y))), **at},
            device_id_type=MESH,
        )

    def await_bytes(ref, sem):
        pltpu.make_async_copy(ref, ref, sem).wait()

    def z_peers(body):
        def step(d, _):
            body(lax.rem(z + d, Z))
            return 0

        lax.fori_loop(1, Z, step, 0)

    def xc_peers(body):
        def step(d, _):
            j = lax.rem(xc + d, XC)
            body(j, j // C, lax.rem(j, C))
            return 0

        lax.fori_loop(1, XC, step, 0)

    def x_peers(body):
        def step(d, _):
            body(lax.rem(x + d, X))
            return 0

        lax.fori_loop(1, X, step, 0)

    barrier = pltpu.get_barrier_semaphore()

    def greet(**at):
        pl.semaphore_signal(
            barrier, inc=1, device_id={**dict(zip(AXES, (z, x, c, y))), **at}, device_id_type=MESH
        )

    z_peers(lambda k: greet(ep_0=k))
    xc_peers(lambda j, a, b: greet(ep_1=a, ep_2=b))
    greet(tp=up1)
    greet(tp=down1)

    weights = [
        pltpu.make_async_copy(src, dst, w_sem.at[i])
        for i, (src, dst) in enumerate(
            ((gate_hbm, gate_v), (up_hbm, up_v), (wo_hbm, wo_v), (down_hbm, down_v))
        )
    ]
    for copy in weights:
        copy.start()

    rows = x_ref[...].astype(f32)
    scale = lax.rsqrt(jnp.mean(rows * rows, axis=-1, keepdims=True) + epsilon)

    def fill(k):
        part = x_ref[:, k * W : (k + 1) * W].astype(f32)
        normed = (part * scale * egain_ref[:, k * W : (k + 1) * W]).astype(bf16)
        zs[k] = dot(place_ref[...], normed).astype(bf16).reshape(zs.shape[1:])
        zr[k, z] = zs[k, z]

    def z_go(k):
        z_peers(
            lambda d: remote(
                zs.at[k, d], zr.at[k, z], z_send.at[k], z_recv.at[k], ep_0=d
            ).start()
        )

    for k in range(NC):
        fill(k)
        if k == 0:
            pl.semaphore_wait(barrier, Z - 1 + XC - 1 + 2)
        z_go(k)

    to_xc = regroup(XC, Z, 2)
    to_z = regroup(Z, XC, 2)

    def step_a(k):
        await_bytes(zr.at[k, pl.ds(0, Z - 1)], z_recv.at[k])
        block = dot(to_xc, zr[k].reshape(-1, W)).astype(bf16)
        xs[k] = block.reshape(xs.shape[1:])
        xc_peers(
            lambda j, a, b: remote(
                xs.at[k, j], arr.at[k, 0, xc], x_send.at[k], x_recv.at[k], ep_1=a, ep_2=b
            ).start()
        )
        arr[k, 0, xc] = xs[k, xc]

    def step_b(k):
        await_bytes(arr.at[k, 0, pl.ds(0, XC - 1)], x_recv.at[k])
        remote(arr.at[k, 0], arr.at[k, 1], y_send.at[k], y_recv.at[k, 0], tp=up1).start()
        remote(arr.at[k, 0], arr.at[k, 2], y_send.at[k], y_recv.at[k, 1], tp=down1).start()

    half = XC // 2

    def step_c(k):
        await_bytes(arr.at[k, 1], y_recv.at[k, 0])
        low = pl.ds(0, half)
        remote(
            arr.at[k, 1, low], arr.at[k, 3, low], y_send.at[k], y_recv.at[k, 2], tp=up1
        ).start()
        await_bytes(arr.at[k, 2], y_recv.at[k, 1])
        high = pl.ds(half, half)
        remote(
            arr.at[k, 2, high], arr.at[k, 3, high], y_send.at[k], y_recv.at[k, 3], tp=down1
        ).start()

    def step_d(k):
        await_bytes(arr.at[k, 3, pl.ds(0, half)], y_recv.at[k, 2])
        await_bytes(arr.at[k, 3, pl.ds(half, half)], y_recv.at[k, 3])
        if k == 0:
            weights[0].wait()
            weights[1].wait()
        tokens = arr[k].reshape(-1, W)
        for acc, w in ((gacc, gate_v), (uacc, up_v)):
            part = dot(tokens, w[k * W : (k + 1) * W, :])
            if k == 0:
                acc[...] = part
            elif k < NC - 1:
                acc[...] += part
            elif acc is gacc:
                gate = acc[...] + part
            else:
                hb[...] = (jax.nn.silu(gate) * (acc[...] + part)).astype(bf16)

    def recurrence():
        shut = jax.nn.sigmoid(-f_ref[...].astype(f32)) * margin_ref[...]
        tri = jnp.where(
            lax.broadcasted_iota(jnp.int32, (seq, seq), 0)
            >= lax.broadcasted_iota(jnp.int32, (seq, seq), 1),
            1.0,
            0.0,
        )
        highest = lax.Precision.HIGHEST
        run_all = jnp.dot(tri, jnp.log1p(-shut), precision=highest, preferred_element_type=f32)
        surges = lax.dot_general(
            tri, surge_ref[...], (((1,), (1,)), ((), ())), precision=highest, preferred_element_type=f32
        )
        causal = lax.broadcasted_iota(jnp.int32, (SPAN, SPAN), 0) >= lax.broadcasted_iota(
            jnp.int32, (SPAN, SPAN), 1
        )
        for h in range(heads):
            cols = slice(h * key, (h + 1) * key)
            run = run_all[:, cols] + surges[:, h : h + 1]
            query = q_ref[:, cols].astype(f32)
            inflow = shut[:, cols]
            value = v_ref[:, cols]
            q_in[h] = (query * jnp.exp(run)).astype(bf16)
            state = None
            for i in range(seq // SPAN):
                at = slice(i * SPAN, (i + 1) * SPAN)
                r, qs, ks, vs = run[at], query[at], inflow[at], value[at]
                mid = r[SPAN // 2 : SPAN // 2 + 1]
                lifted = (qs * jnp.exp(r - mid)).astype(bf16)
                lowered = (ks * jnp.exp(mid - r)).astype(bf16)
                scores = jnp.where(causal, dot_nt(lifted, lowered), 0.0)
                out = dot(scores.astype(bf16), vs)
                close = r[SPAN - 1 : SPAN]
                added = dot_tn(vs, (ks * jnp.exp(close - r)).astype(bf16))
                if state is None:
                    state = added
                else:
                    before = run[i * SPAN - 1 : i * SPAN]
                    out = out + dot_nt((qs * jnp.exp(r - before)).astype(bf16), state.astype(bf16))
                    state = jnp.exp(close - before) * state + added
                local_out[at, cols] = out
            s1[c, h, pl.ds(0, key)] = state.astype(bf16)
            s1[c, h, pl.ds(key, 16)] = totals_rows(run[seq - 1 : seq])
        remote(s1.at[c], s1.at[c], s_send.at[0], s_recv.at[0], ep_2=1 - c).start()

    empty = lambda n: (jnp.zeros((n, key), f32), jnp.zeros((1, key), f32))

    def state_2():
        await_bytes(s1.at[1 - c], s_recv.at[0])
        both = chain(read_state(s1, (0, c), key), read_state(s1, (1, c), key))
        s2[x, pl.ds(0, key)] = both[0].astype(bf16)
        s2[x, pl.ds(key, 16)] = totals_rows(both[1])
        x_peers(
            lambda a: remote(s2.at[x], s2.at[x], s_send.at[1], s_recv.at[1], ep_1=a).start()
        )

    def x_prefix():
        prefix = empty(key)
        total = empty(key)
        for i in range(X):
            total = chain(total, read_state(s2, (i,), key))
            if i < X - 1:
                prefix = keep_if(i + 1 == x, total, prefix)
        return prefix, total

    def state_3():
        await_bytes(s2.at[pl.ds(0, X - 1)], s_recv.at[1])
        _, total = x_prefix()
        mine = total[0][:quarter]
        for i in range(1, X):
            mine = jnp.where(x == i, total[0][i * quarter : (i + 1) * quarter], mine)
        s3[z, pl.ds(0, quarter)] = mine.astype(bf16)
        s3[z, pl.ds(quarter, 16)] = totals_rows(total[1])
        z_peers(
            lambda k: remote(s3.at[z], s3.at[z], s_send.at[2], s_recv.at[2], ep_0=k).start()
        )

    def state_4():
        await_bytes(s3.at[pl.ds(0, Z - 1)], s_recv.at[2])
        prefix = empty(quarter)
        total = empty(quarter)
        for i in range(Z - 1):
            total = chain(total, read_state(s3, (i,), quarter))
            prefix = keep_if(i + 1 == z, total, prefix)
        s4[x] = prefix[0].astype(bf16)
        x_peers(
            lambda a: remote(s4.at[x], s4.at[x], s_send.at[3], s_recv.at[3], ep_1=a).start()
        )

    def state_5():
        await_bytes(s4.at[pl.ds(0, X - 1)], s_recv.at[3])
        before = s4[...].astype(f32).reshape(key, key)
        prefix, _ = x_prefix()
        s5[c] = (jnp.exp(prefix[1]) * before + prefix[0]).astype(bf16)
        remote(s5.at[c], s5.at[c], s_send.at[4], s_recv.at[4], ep_2=1 - c).start()

    def mix():
        await_bytes(s5.at[1 - c], s_recv.at[4])
        for h in range(heads):
            cols = slice(h * key, (h + 1) * key)
            chip = s5[h].astype(f32)
            first = read_state(s1, (0, h), key)
            entering = jnp.where(c == 0, chip, jnp.exp(first[1]) * chip + first[0])
            out = local_out[:, cols] + dot_nt(q_in[h], entering.astype(bf16))
            out = out * lax.rsqrt(jnp.mean(out * out, axis=-1, keepdims=True) + epsilon)
            gate = og_ref[:, cols].astype(f32)
            ha[:, cols] = (out * hgain_ref[:, cols] * jax.nn.silu(gate)).astype(bf16)
        weights[2].wait()
        for k in range(NC):
            at = slice(k * W, (k + 1) * W)
            mp[:, :, :, at] = dot(ha[...], wo_v[:, at]).astype(bf16).reshape(mp.shape[:3] + (W,))

    def mix_a():
        remote(mp.at[across, 0], m1.at[0], m_send.at[0], m_recv.at[0], tp=up1).start()
        remote(mp.at[across, 1], m1.at[1], m_send.at[0], m_recv.at[1], tp=down1).start()

    def mix_b():
        for i, to in ((0, up1), (1, down1)):
            await_bytes(m1.at[i], m_recv.at[i])
            mp[to, i] = (mp[to, i].astype(f32) + m1[i].astype(f32)).astype(bf16)
            remote(mp.at[to], m2.at[i], m_send.at[1], m_recv.at[2 + i], tp=to).start()

    def mix_c():
        await_bytes(m2.at[0], m_recv.at[2])
        await_bytes(m2.at[1], m_recv.at[3])
        total = mp[y].astype(f32) + m2[0].astype(f32) + m2[1].astype(f32)
        mixed_ref[...] = total.astype(bf16).reshape(mixed_ref.shape)

    def step_e(k):
        if k == 0:
            weights[3].wait()
        part = dot(hb[...], down_v[:, k * W : (k + 1) * W])
        ps[k] = part.astype(bf16).reshape(ps.shape[1:])
        remote(ps.at[k, 3, 0], r1.at[k, 0], ra_send.at[k], r_recv.at[k, 0], tp=up1).start()
        remote(ps.at[k, 3, 1], r1.at[k, 1], ra_send.at[k], r_recv.at[k, 1], tp=down1).start()

    def step_f(k):
        for i, rel, to in ((0, 2, up1), (1, 1, down1)):
            await_bytes(r1.at[k, i], r_recv.at[k, i])
            ps[k, rel, i] = (ps[k, rel, i].astype(f32) + r1[k, i].astype(f32)).astype(bf16)
            remote(ps.at[k, rel], r2.at[k, i], rb_send.at[k], r_recv.at[k, 2 + i], tp=to).start()

    def step_g(k):
        await_bytes(r2.at[k, 0], r_recv.at[k, 2])
        await_bytes(r2.at[k, 1], r_recv.at[k, 3])
        total = ps[k, 0].astype(f32) + r2[k, 0].astype(f32) + r2[k, 1].astype(f32)
        rx[k] = total.astype(bf16).reshape(rx.shape[1:])
        xc_peers(
            lambda j, a, b: remote(
                rx.at[k, j], xb.at[k, xc], rx_send.at[k], rx_recv.at[k], ep_1=a, ep_2=b
            ).start()
        )
        xb[k, xc] = rx[k, xc]

    def step_h(k):
        await_bytes(xb.at[k, pl.ds(0, XC - 1)], rx_recv.at[k])
        block = dot(to_z, xb[k].reshape(-1, W)).astype(bf16)
        rzs[k] = block.reshape(rzs.shape[1:])
        z_peers(
            lambda d: remote(
                rzs.at[k, d], rzr.at[k, z], rz_send.at[k], rz_recv.at[k], ep_0=d
            ).start()
        )
        rzr[k, z] = rzs[k, z]

    comb_hi = comb_ref[...].astype(bf16)
    comb_lo = (comb_ref[...] - comb_hi.astype(f32)).astype(bf16)

    def step_i(k):
        await_bytes(rzr.at[k, pl.ds(0, Z - 1)], rz_recv.at[k])
        results = rzr[k].reshape(-1, W)
        moe_ref[:, k * W : (k + 1) * W] = (dot(comb_hi, results) + dot(comb_lo, results)).astype(bf16)

    recurrence()
    side = {0: state_2, 1: state_3, 3: state_4, 4: state_5, 5: mix}
    last = NC + 3
    for t in range(last):
        if t < NC:
            step_a(t)
        if 0 <= t - 1 < NC:
            step_b(t - 1)
        if t - 1 == NC - 1:
            mix_a()
        if 0 <= t - 2 < NC:
            step_c(t - 2)
        if t - 2 == NC - 1:
            mix_b()
        if 0 <= t - 3 < NC:
            step_d(t - 3)
        if t in side:
            side[t]()
    for t in range(NC + 4):
        if t < NC:
            step_e(t)
        if 0 <= t - 1 < NC:
            step_f(t - 1)
        if 0 <= t - 2 < NC:
            step_g(t - 2)
        if 0 <= t - 3 < NC:
            step_h(t - 3)
        if 0 <= t - 4 < NC:
            step_i(t - 4)
        if t == 2:
            mix_c()

    for k in range(NC):
        await_bytes(zs.at[k, pl.ds(0, Z - 1)], z_send.at[k])
        await_bytes(xs.at[k, pl.ds(0, XC - 1)], x_send.at[k])
        await_bytes(arr.at[k, pl.ds(0, 3)], y_send.at[k])
        await_bytes(ps.at[k, 3], ra_send.at[k])
        await_bytes(ps.at[k, pl.ds(1, 2)], rb_send.at[k])
        await_bytes(rx.at[k, pl.ds(0, XC - 1)], rx_send.at[k])
        await_bytes(rzs.at[k, pl.ds(0, Z - 1)], rz_send.at[k])
    await_bytes(mp.at[0], m_send.at[0])
    await_bytes(mp.at[pl.ds(0, 2)], m_send.at[1])
    await_bytes(s1.at[0], s_send.at[0])
    await_bytes(s2.at[pl.ds(0, X - 1)], s_send.at[1])
    await_bytes(s3.at[pl.ds(0, Z - 1)], s_send.at[2])
    await_bytes(s4.at[pl.ds(0, X - 1)], s_send.at[3])
    await_bytes(s5.at[0], s_send.at[4])


def slot_tables(block_routes, logits, experts):
    chosen = block_routes.reshape(-1)
    table = (chosen[:, None] == jnp.arange(experts, dtype=jnp.int32)[None, :]).astype(jnp.int32)
    before = jnp.cumsum(table, axis=0) - table
    slot = chosen * 2 + jnp.sum(before * table, axis=1)
    taken = slot[:, None] == jnp.arange(2 * experts, dtype=jnp.int32)[None, :]
    weight = jax.nn.softmax(logits, axis=-1).reshape(-1)
    tokens = block_routes.shape[0]
    place = jnp.any(taken.reshape(tokens, TOP, -1), axis=1).astype(bf16).T
    comb = jnp.sum(jnp.where(taken, weight[:, None], 0.0).reshape(tokens, TOP, -1), axis=1)
    return place, comb


def per_device(
    sizes,
    recurrence_query,
    forget_preactivation,
    recurrence_value,
    output_gate_preactivation,
    forget_margin,
    surge_log_decay,
    head_norm_gain,
    recurrence_output_matrix,
    second_micro_input,
    expert_norm_gain,
    routes,
    router_chosen_logits,
    expert_gate_matrix,
    expert_up_matrix,
    expert_down_matrix,
):
    Z, X, C, Y, NC = sizes
    XC = X * C
    experts = Z * XC
    tokens, D = second_micro_input.shape
    seq, width = recurrence_query.shape
    heads = surge_log_decay.shape[0]
    key = width // heads
    F = expert_gate_matrix.shape[2]
    W = D // NC
    own_routes = lax.dynamic_slice_in_dim(routes, lax.axis_index("tp") * tokens, tokens, 0)
    place, comb = slot_tables(own_routes, router_chosen_logits, experts)
    slots = 2 * experts
    V = pltpu.VMEM
    DMA = pltpu.SemaphoreType.DMA
    scratch = [
        V((NC, Z, 2 * XC, W), bf16),
        V((NC, Z, 2 * XC, W), bf16),
        V((NC, XC, 2 * Z, W), bf16),
        V((NC, Y, XC, 2 * Z, W), bf16),
        V((D, F), bf16),
        V((D, F), bf16),
        V((F, D), bf16),
        V((width, D), bf16),
        V((Y * slots, F), f32),
        V((Y * slots, F), f32),
        V((Y * slots, F), bf16),
        V((NC, Y, 2, slots // 2, W), bf16),
        V((NC, 2, slots // 2, W), bf16),
        V((NC, 2, 2, slots // 2, W), bf16),
        V((NC, XC, 2 * Z, W), bf16),
        V((NC, XC, 2 * Z, W), bf16),
        V((NC, Z, 2 * XC, W), bf16),
        V((NC, Z, 2 * XC, W), bf16),
        V((Y, 2, seq // Y // 2, D), bf16),
        V((2, seq // Y // 2, D), bf16),
        V((2, 2, seq // Y // 2, D), bf16),
        V((C, heads, key + 16, key), bf16),
        V((X, key + 16, key), bf16),
        V((Z, key // X + 16, key), bf16),
        V((X, key // X, key), bf16),
        V((C, key, key), bf16),
        V((seq, width), f32),
        V((heads, seq, key), bf16),
        V((seq, width), bf16),
        DMA((4,)),
        DMA((NC,)),
        DMA((NC,)),
        DMA((NC,)),
        DMA((NC,)),
        DMA((NC,)),
        DMA((NC, 4)),
        DMA((NC,)),
        DMA((NC,)),
        DMA((NC, 4)),
        DMA((NC,)),
        DMA((NC,)),
        DMA((NC,)),
        DMA((NC,)),
        DMA((2,)),
        DMA((4,)),
        DMA((5,)),
        DMA((5,)),
    ]
    vmem = pl.BlockSpec(memory_space=pltpu.VMEM)
    hbm = pl.BlockSpec(memory_space=pl.ANY)
    out = jax.ShapeDtypeStruct((tokens, D), bf16)
    return pl.pallas_call(
        functools.partial(kernel, sizes),
        out_shape=(jax.ShapeDtypeStruct((seq // Y, D), bf16), out),
        in_specs=[vmem] * 11 + [hbm] * 4,
        out_specs=(vmem, vmem),
        scratch_shapes=scratch,
        compiler_params=pltpu.CompilerParams(
            collective_id=0, has_side_effects=True, vmem_limit_bytes=63 * 1024 * 1024
        ),
    )(
        recurrence_query,
        forget_preactivation,
        recurrence_value,
        output_gate_preactivation,
        forget_margin.reshape(1, -1),
        surge_log_decay,
        head_norm_gain.reshape(1, -1),
        second_micro_input,
        expert_norm_gain.reshape(1, -1),
        place,
        comb,
        recurrence_output_matrix,
        expert_gate_matrix[0],
        expert_up_matrix[0],
        expert_down_matrix[0],
    )


def build(finer, chunks):
    sizes = tuple(finer.shape[a] for a in AXES) + (chunks,)
    in_specs = (
        P(EP, "tp"),
        P(EP, "tp"),
        P(EP, "tp"),
        P(EP, "tp"),
        P("tp"),
        P("tp", EP),
        P("tp"),
        P("tp", None),
        P(EP_TP, None),
        P(),
        P(EP, None),
        P(EP_TP, None),
        P(EP, None, "tp"),
        P(EP, None, "tp"),
        P(EP, "tp", None),
    )
    out_specs = (P(EP_TP, None), P(EP_TP, None))
    return jax.shard_map(
        functools.partial(per_device, sizes),
        mesh=finer,
        in_specs=in_specs,
        out_specs=out_specs,
        check_vma=False,
    )


def solution(mesh):
    return build(Mesh(mesh.devices.reshape(8, 4, 2, mesh.shape["tp"]), AXES), CHUNKS)
```

time: 284 us -> 139 us (0.49)
  blocking collectives: 154 us -> 0 us
  Pallas kernels: 0 us -> 123 us
  waiting for transfers between devices: 26.2 us -> 0 us
  matrix products: 22.1 us -> 0 us
  local copies, waits for them, and re-layouts: 34 us -> 12.1 us
  starting transfers between devices: 17.1 us -> 0 us
  between operations: 14.5 us -> 0.69 us
  other arithmetic: 15.1 us -> 3.23 us
    pallas_call x0 -> x1, Pallas kernels: none -> 123 us  [per_device(): pl.pallas_call(functools.partial(kernel, sizes), out_shape=(jax.ShapeDtyp...]
    all_to_all x2 -> x0, blocking collectives: 96.3 us -> none  [the longest x1 54.9 us: sum_at_owner(): lax.all_to_all(tiles, axis, split_axis=0, concat_axis=0, tiled=True)]
    all_gather x6 -> x0, blocking collectives: 57.3 us -> none  [carried_in(): lax.all_gather(part.astype(kind), axis)]
    all_to_all x1 -> x0, waiting for transfers between devices: 26.2 us -> none  [per_device(): lax.all_to_all(expert_rows.reshape(expert_count, capacity, width), EP, sp...]
    dot_general x17 -> x0, matrix products: 22.1 us -> none  [the longest x1 4.91 us: expert_hidden(): jnp.dot(flat_rows, gate_local, preferred_element_type=jnp.float32)]
    all_to_all x1 -> x0, starting transfers between devices: 17.1 us -> none  [per_device(): lax.all_to_all(expert_rows.reshape(expert_count, capacity, width), EP, sp...]
    reshape x6 -> x0, local copies, waits for them, and re-layouts: 15.7 us -> none  [the longest x1 7.24 us: per_device(): piece.reshape(piece_count * slot_count, width)]
    unnamed x41 -> x9, local copies, waits for them, and re-layouts: 2.61 us -> 11 us
  transfers between devices with their start and end apart: 2 -> 0, of which waited for: 1 -> 0; matrix products, arithmetic and copies ran while one was open for 7% -> 0% of each run, Pallas kernels for 0% -> 0%
where the time goes in v1:
time: 139 us
  Pallas kernels  123 us (88%)
  local copies, waits for them, and re-layouts  12.1 us (9%)
  other arithmetic  3.23 us (2%)
    pallas_call x1, Pallas kernels, per_device(): pl.pallas_call(functools.partial(kernel, sizes), out_shape=(jax.ShapeDtyp...  123 us
    unnamed x9, local copies, waits for them, and re-layouts  11 us

profile of v1, /device:TPU:1, one launch (start us, length us, event | category | flops | bytes accessed | tf_op | source)
XLA Modules:
  0.0 138.7 jit_solution(17812735511883897934)
XLA Ops:
  0.6 0.0 copy-start
  0.6 0.7 reduce_max.9
  1.3 0.7 fusion.3
  2.0 0.7 fusion.2
  2.7 0.0 copy-done
  2.7 0.1 constant_dynamic-slice_fusion
  2.8 0.1 copy.35
  2.9 0.1 eq.30
  3.0 0.1 fusion.1
  3.1 0.1 reduce_window_sum.11
  3.2 0.2 select_reduce_fusion.1
  3.4 0.1 reduce_sum.30
  3.5 0.1 copy.31
  3.6 0.1 fusion
  3.7 0.7 select_reduce_fusion.comb_ref
  4.4 0.7 copy.32
  5.1 0.0 copy-start.1
  5.1 4.7 %copy.33 = bf16[1,4096,352]{2,1,0:T(8,128)(2,1)} copy(bf16[1,4096,352]{1,2,0:T(8,128)(2,1)} %param.27) | data formatting | bytes 5767168 | tf_op args[12]
  9.8 0.0 copy-done.1
  9.8 2.8 %copy.34 = bf16[1,4096,352]{2,1,0:T(8,128)(2,1)} copy(bf16[1,4096,352]{1,2,0:T(8,128)(2,1)S(1)} %copy-done.1) | data formatting | bytes 5767168 | tf_op args[13]
  12.6 122.7 %shard_map.158 = (bf16[32,4096]{1,0:T(8,128)(2,1)}, bf16[32,4096]{1,0:T(8,128)(2,1)}) custom-call(bf16[128,256]{1,0:T(8,128)(2,1)} %q_ref.1, bf16[128,256]{1,0:T(8,128)(2,1)} %f_ref.1, bf16[128,256]{1,0:T(8,128)(2,1)} %v_ref.1, bf16[128,256]{1,0:T(8,128)(2,1)} %og_ref.1, f32[1,256]{1,0:T(1,128)} %bitcast.12, f32[2,128]{1,0:T(2,128)} %surge_ref.1, ...), custom_call_target="tpu_custom_call" | custom-call | tf_op jit(solution)/shard_map/pallas_call | solution.py:543
  135.4 1.7 %copy.38 = bf16[32,4096]{1,0:T(8,128)(2,1)} copy(bf16[32,4096]{1,0:T(8,128)(2,1)} %get-tuple-element.4) | data formatting | bytes 524288
  137.1 1.7 %copy.39 = bf16[32,4096]{1,0:T(8,128)(2,1)} copy(bf16[32,4096]{1,0:T(8,128)(2,1)} %get-tuple-element.5) | data formatting | bytes 524288
  (2 shorter events, 0.0 us)
Async XLA Ops:
  0.6 2.1 %copy-start = (s32[128,2]{0,1:T(2,128)S(1)}, s32[128,2]{0,1:T(2,128)}, u32[]{:S(2)}) copy-start(s32[128,2]{0,1:T(2,128)} %param.25) | copy-start | bytes 3076
  5.1 4.7 %copy-start.1 = (bf16[1,4096,352]{1,2,0:T(8,128)(2,1)S(1)}, bf16[1,4096,352]{1,2,0:T(8,128)(2,1)}, u32[]{:S(2)}) copy-start(bf16[1,4096,352]{1,2,0:T(8,128)(2,1)} %param.28) | copy-start | bytes 8650756

commit v2 on v1

--- a/solution.py
+++ b/solution.py
@@ -73,7 +73,7 @@
 
 def kernel(
     sizes,
-    q_ref, f_ref, v_ref, og_ref, margin_ref, surge_ref, hgain_ref, x_ref, egain_ref, place_ref, comb_ref,
+    q_ref, f_ref, v_ref, og_ref, margin_ref, surge_ref, hgain_ref, x_ref, egain_ref, routes_ref, logits_ref,
     wo_hbm, gate_hbm, up_hbm, down_hbm,
     mixed_ref, moe_ref,
     zs, zr, xs, arr, gate_v, up_v, down_v, wo_v, gacc, uacc, hb, ps, r1, r2, rx, xb, rzs, rzr,
@@ -92,6 +92,10 @@
     quarter = s4.shape[1]
     up1, down1, across = lax.rem(y + 1, Y), lax.rem(y + Y - 1, Y), lax.rem(y + 2, Y)
 
+    z_at = [lax.rem(z + d, Z) for d in range(Z)]
+    xc_at = [lax.rem(xc + d, XC) for d in range(XC)]
+    xc_at = [(j, j // C, lax.rem(j, C)) for j in xc_at]
+
     def remote(src, dst, send, recv, **at):
         return pltpu.make_async_remote_copy(
             src_ref=src,
@@ -106,26 +110,16 @@
         pltpu.make_async_copy(ref, ref, sem).wait()
 
     def z_peers(body):
-        def step(d, _):
-            body(lax.rem(z + d, Z))
-            return 0
-
-        lax.fori_loop(1, Z, step, 0)
+        for d in range(1, Z):
+            body(z_at[d])
 
     def xc_peers(body):
-        def step(d, _):
-            j = lax.rem(xc + d, XC)
-            body(j, j // C, lax.rem(j, C))
-            return 0
-
-        lax.fori_loop(1, XC, step, 0)
+        for d in range(1, XC):
+            body(*xc_at[d])
 
     def x_peers(body):
-        def step(d, _):
+        for d in range(1, X):
             body(lax.rem(x + d, X))
-            return 0
-
-        lax.fori_loop(1, X, step, 0)
 
     barrier = pltpu.get_barrier_semaphore()
 
@@ -148,13 +142,18 @@
     for copy in weights:
         copy.start()
 
+    tokens = x_ref.shape[0]
+    chosen = routes_ref[:, :tokens]
+    for i in range(1, Y):
+        chosen = jnp.where(y == i, routes_ref[:, i * tokens : (i + 1) * tokens], chosen)
+    place, comb = slot_tables(chosen, logits_ref[...], Z * XC)
     rows = x_ref[...].astype(f32)
     scale = lax.rsqrt(jnp.mean(rows * rows, axis=-1, keepdims=True) + epsilon)
 
     def fill(k):
         part = x_ref[:, k * W : (k + 1) * W].astype(f32)
         normed = (part * scale * egain_ref[:, k * W : (k + 1) * W]).astype(bf16)
-        zs[k] = dot(place_ref[...], normed).astype(bf16).reshape(zs.shape[1:])
+        zs[k] = dot(place, normed).astype(bf16).reshape(zs.shape[1:])
         zr[k, z] = zs[k, z]
 
     def z_go(k):
@@ -211,7 +210,7 @@
             weights[1].wait()
         tokens = arr[k].reshape(-1, W)
         for acc, w in ((gacc, gate_v), (uacc, up_v)):
-            part = dot(tokens, w[k * W : (k + 1) * W, :])
+            part = dot_nt(tokens, w[:, k * W : (k + 1) * W])
             if k == 0:
                 acc[...] = part
             elif k < NC - 1:
@@ -386,8 +385,9 @@
         )
         rzr[k, z] = rzs[k, z]
 
-    comb_hi = comb_ref[...].astype(bf16)
-    comb_lo = (comb_ref[...] - comb_hi.astype(f32)).astype(bf16)
+    comb = comb.T
+    comb_hi = comb.astype(bf16)
+    comb_lo = (comb - comb_hi.astype(f32)).astype(bf16)
 
     def step_i(k):
         await_bytes(rzr.at[k, pl.ds(0, Z - 1)], rz_recv.at[k])
@@ -395,36 +395,42 @@
         moe_ref[:, k * W : (k + 1) * W] = (dot(comb_hi, results) + dot(comb_lo, results)).astype(bf16)
 
     recurrence()
-    side = {0: state_2, 1: state_3, 3: state_4, 4: state_5, 5: mix}
-    last = NC + 3
-    for t in range(last):
+    for t in range(NC + 3):
         if t < NC:
             step_a(t)
+        if t == NC + 1:
+            mix()
         if 0 <= t - 1 < NC:
             step_b(t - 1)
-        if t - 1 == NC - 1:
-            mix_a()
         if 0 <= t - 2 < NC:
             step_c(t - 2)
-        if t - 2 == NC - 1:
-            mix_b()
+        if t == NC + 1:
+            mix_a()
+        if t == 0:
+            state_2()
+        if t == 1:
+            state_3()
+        if t == NC:
+            state_4()
         if 0 <= t - 3 < NC:
             step_d(t - 3)
-        if t in side:
-            side[t]()
+        if t == NC:
+            state_5()
     for t in range(NC + 4):
         if t < NC:
             step_e(t)
         if 0 <= t - 1 < NC:
             step_f(t - 1)
+        if t == NC:
+            mix_b()
         if 0 <= t - 2 < NC:
             step_g(t - 2)
         if 0 <= t - 3 < NC:
             step_h(t - 3)
+        if t == NC + 2:
+            mix_c()
         if 0 <= t - 4 < NC:
             step_i(t - 4)
-        if t == 2:
-            mix_c()
 
     for k in range(NC):
         await_bytes(zs.at[k, pl.ds(0, Z - 1)], z_send.at[k])
@@ -443,17 +449,31 @@
     await_bytes(s5.at[0], s_send.at[4])
 
 
-def slot_tables(block_routes, logits, experts):
-    chosen = block_routes.reshape(-1)
-    table = (chosen[:, None] == jnp.arange(experts, dtype=jnp.int32)[None, :]).astype(jnp.int32)
-    before = jnp.cumsum(table, axis=0) - table
-    slot = chosen * 2 + jnp.sum(before * table, axis=1)
-    taken = slot[:, None] == jnp.arange(2 * experts, dtype=jnp.int32)[None, :]
-    weight = jax.nn.softmax(logits, axis=-1).reshape(-1)
-    tokens = block_routes.shape[0]
-    place = jnp.any(taken.reshape(tokens, TOP, -1), axis=1).astype(bf16).T
-    comb = jnp.sum(jnp.where(taken, weight[:, None], 0.0).reshape(tokens, TOP, -1), axis=1)
-    return place, comb
+def slot_tables(chosen, logits, experts):
+    tokens = chosen.shape[1]
+    top = jnp.max(logits, axis=0, keepdims=True)
+    raised = jnp.exp(logits - top)
+    weight = raised / jnp.sum(raised, axis=0, keepdims=True)
+    expert = lax.broadcasted_iota(jnp.int32, (experts, tokens), 0)
+    named = [jnp.where(expert == chosen[j : j + 1], 1.0, 0.0) for j in range(TOP)]
+    earlier = lax.broadcasted_iota(jnp.int32, (tokens, tokens), 0) < lax.broadcasted_iota(
+        jnp.int32, (tokens, tokens), 1
+    )
+    before = dot(sum(named).astype(bf16), jnp.where(earlier, 1.0, 0.0).astype(bf16))
+    row = lax.broadcasted_iota(jnp.int32, (2 * experts, tokens), 0).astype(f32)
+    place = jnp.zeros((2 * experts, tokens), f32)
+    comb = place
+    for j in range(TOP):
+        rank = jnp.sum(named[j] * before, axis=0, keepdims=True)
+        here = row == 2.0 * chosen[j : j + 1].astype(f32) + rank
+        place = jnp.where(here, 1.0, place)
+        comb = jnp.where(here, weight[j : j + 1], comb)
+    return place.astype(bf16), comb
+
+
+def hand_on(mixed_in, moe_in, mixed_out, moe_out):
+    mixed_out[...] = mixed_in[...]
+    moe_out[...] = moe_in[...]
 
 
 def per_device(
@@ -483,8 +503,6 @@
     key = width // heads
     F = expert_gate_matrix.shape[2]
     W = D // NC
-    own_routes = lax.dynamic_slice_in_dim(routes, lax.axis_index("tp") * tokens, tokens, 0)
-    place, comb = slot_tables(own_routes, router_chosen_logits, experts)
     slots = 2 * experts
     V = pltpu.VMEM
     DMA = pltpu.SemaphoreType.DMA
@@ -493,8 +511,8 @@
         V((NC, Z, 2 * XC, W), bf16),
         V((NC, XC, 2 * Z, W), bf16),
         V((NC, Y, XC, 2 * Z, W), bf16),
-        V((D, F), bf16),
-        V((D, F), bf16),
+        V((F, D), bf16),
+        V((F, D), bf16),
         V((F, D), bf16),
         V((width, D), bf16),
         V((Y * slots, F), f32),
@@ -540,7 +558,7 @@
     vmem = pl.BlockSpec(memory_space=pltpu.VMEM)
     hbm = pl.BlockSpec(memory_space=pl.ANY)
     out = jax.ShapeDtypeStruct((tokens, D), bf16)
-    return pl.pallas_call(
+    results = pl.pallas_call(
         functools.partial(kernel, sizes),
         out_shape=(jax.ShapeDtypeStruct((seq // Y, D), bf16), out),
         in_specs=[vmem] * 11 + [hbm] * 4,
@@ -559,13 +577,19 @@
         head_norm_gain.reshape(1, -1),
         second_micro_input,
         expert_norm_gain.reshape(1, -1),
-        place,
-        comb,
+        routes.T,
+        router_chosen_logits.T,
         recurrence_output_matrix,
-        expert_gate_matrix[0],
-        expert_up_matrix[0],
+        expert_gate_matrix[0].T,
+        expert_up_matrix[0].T,
         expert_down_matrix[0],
     )
+    return pl.pallas_call(
+        hand_on,
+        out_shape=(jax.ShapeDtypeStruct((seq // Y, D), bf16), out),
+        in_specs=[vmem] * 2,
+        out_specs=(vmem, vmem),
+    )(*results)
 
 
 def build(finer, chunks):

time: 139 us -> 117 us (0.84)
  local copies, waits for them, and re-layouts: 12.1 us -> 0 us
  Pallas kernels: 123 us -> 117 us
  other arithmetic: 3.23 us -> 0 us
    unnamed x9 -> x0, local copies, waits for them, and re-layouts: 11 us -> none
    pallas_call x1, Pallas kernels: 123 us -> 115 us  [per_device(): pl.pallas_call(functools.partial(kernel, sizes), out_shape=(jax.ShapeDtyp...]
    pallas_call x0 -> x1, Pallas kernels: none -> 1.84 us  [per_device(): pl.pallas_call(hand_on, out_shape=(jax.ShapeDtypeStruct((seq // Y, D), bf...]
    reduce_sum x3 -> x0, other arithmetic: 1.57 us -> none  [the longest x1 0.7 us: slot_tables(): weight = jax.nn.softmax(logits, axis=-1).reshape(-1)]
where the time goes in v2:
time: 117 us
  Pallas kernels  117 us (100%)
    pallas_call x1, Pallas kernels, per_device(): pl.pallas_call(functools.partial(kernel, sizes), out_shape=(jax.ShapeDtyp...  115 us

profile of v2, /device:TPU:1, one launch (start us, length us, event | category | flops | bytes accessed | tf_op | source)
XLA Modules:
  0.0 117.3 jit_solution(11617041978027826616)
XLA Ops:
  0.6 114.8 %shard_map.158 = (bf16[32,4096]{1,0:T(8,128)(2,1)}, bf16[32,4096]{1,0:T(8,128)(2,1)}) custom-call(bf16[128,256]{1,0:T(8,128)(2,1)} %q_ref.1, bf16[128,256]{1,0:T(8,128)(2,1)} %f_ref.1, bf16[128,256]{1,0:T(8,128)(2,1)} %v_ref.1, bf16[128,256]{1,0:T(8,128)(2,1)} %og_ref.1, f32[1,256]{1,0:T(1,128)} %bitcast.16, f32[2,128]{1,0:T(2,128)} %surge_ref.1, ...), custom_call_target="tpu_custom_call" | custom-call | tf_op jit(solution)/shard_map/pallas_call | solution.py:561
  115.4 1.8 %shard_map.159 = (bf16[32,4096]{1,0:T(8,128)(2,1)}, bf16[32,4096]{1,0:T(8,128)(2,1)}) custom-call(bf16[32,4096]{1,0:T(8,128)(2,1)} %get-tuple-element.4.mixed_in, bf16[32,4096]{1,0:T(8,128)(2,1)} %get-tuple-element.5.moe_in), custom_call_target="tpu_custom_call" | custom-call | tf_op jit(solution)/shard_map/pallas_call | solution.py:587

commit v3 on v2

--- a/solution.py
+++ b/solution.py
@@ -10,7 +10,11 @@
 
 TOP = 2
 SPAN = 64
-CHUNKS = 8
+CHUNKS = (1,) * 15
+WIDE_AT = (1, 6, -1, 2)
+WIDE = 1
+OUT_LAGS = (3, 6, 9)
+BACK_LAGS = (3, 6, 8, 11)
 AXES = ("ep_0", "ep_1", "ep_2", "tp")
 EP = ("ep_0", "ep_1", "ep_2")
 EP_TP = AXES
@@ -73,22 +77,45 @@
 
 def kernel(
     sizes,
-    q_ref, f_ref, v_ref, og_ref, margin_ref, surge_ref, hgain_ref, x_ref, egain_ref, routes_ref, logits_ref,
+    q_hbm, f_hbm, v_hbm, og_hbm, margin_ref, surge_ref, hgain_ref, x_hbm, egain_ref, routes_ref, logits_ref,
     wo_hbm, gate_hbm, up_hbm, down_hbm,
     mixed_ref, moe_ref,
     zs, zr, xs, arr, gate_v, up_v, down_v, wo_v, gacc, uacc, hb, ps, r1, r2, rx, xb, rzs, rzr,
     mp, m1, m2, s1, s2, s3, s4, s5, local_out, q_in, ha,
-    w_sem, z_send, z_recv, x_send, x_recv, y_send, y_recv,
+    tk, zsq, zrq, xsq, arrq, psq, xbq, rzsq, rzrq, uq, t1, t2, lg, q_send, q_recv,
+    q_ref, f_ref, v_ref, og_ref, x_ref, in_sem, w_sem, z_send, z_recv, x_send, x_recv, y_send, y_recv,
     ra_send, rb_send, r_recv, rx_send, rx_recv, rz_send, rz_recv,
     m_send, m_recv, s_send, s_recv,
 ):
-    Z, X, C, Y, NC = sizes
+    Z, X, C, Y, widths = sizes
+    NC = len(widths)
+    starts = [sum(widths[:k]) for k in range(NC)]
+    wide = slice(sum(widths), x_ref.shape[1])
+    wq = x_ref.shape[1] - sum(widths)
     XC = X * C
     z, x, c, y = (lax.axis_index(a) for a in AXES)
     xc = x * C + c
-    W = zs.shape[3]
+
+    def of(ref, k, *index):
+        index = (k,) + index
+        rest = (slice(None),) * (len(ref.shape) - 1 - len(index))
+        if widths[k] == ref.shape[-1]:
+            return ref.at[index]
+        return ref.at[index + rest + (pl.ds(0, widths[k]),)]
+
+    def columns(k):
+        return slice(starts[k], starts[k] + widths[k])
+
     heads, key = surge_ref.shape[0], s4.shape[2]
     seq = q_ref.shape[0]
+    inputs = [
+        pltpu.make_async_copy(src, dst, in_sem.at[i])
+        for i, (src, dst) in enumerate(
+            ((x_hbm, x_ref), (f_hbm, f_ref), (q_hbm, q_ref), (v_hbm, v_ref), (og_hbm, og_ref))
+        )
+    ]
+    for copy in inputs:
+        copy.start()
     quarter = s4.shape[1]
     up1, down1, across = lax.rem(y + 1, Y), lax.rem(y + Y - 1, Y), lax.rem(y + 2, Y)
 
@@ -143,23 +170,124 @@
         copy.start()
 
     tokens = x_ref.shape[0]
-    chosen = routes_ref[:, :tokens]
-    for i in range(1, Y):
-        chosen = jnp.where(y == i, routes_ref[:, i * tokens : (i + 1) * tokens], chosen)
-    place, comb = slot_tables(chosen, logits_ref[...], Z * XC)
+
+    def tables(owner, logits):
+        chosen = routes_ref[:, :tokens]
+        for i in range(1, Y):
+            chosen = jnp.where(owner == i, routes_ref[:, i * tokens : (i + 1) * tokens], chosen)
+        return slot_tables(chosen, logits, Z * XC)
+
+    owners = (y, down1, up1, across)
+    place, comb = tables(y, logits_ref[...])
+    inputs[0].wait()
     rows = x_ref[...].astype(f32)
     scale = lax.rsqrt(jnp.mean(rows * rows, axis=-1, keepdims=True) + epsilon)
 
     def fill(k):
-        part = x_ref[:, k * W : (k + 1) * W].astype(f32)
-        normed = (part * scale * egain_ref[:, k * W : (k + 1) * W]).astype(bf16)
-        zs[k] = dot(place, normed).astype(bf16).reshape(zs.shape[1:])
-        zr[k, z] = zs[k, z]
+        part = x_ref[:, columns(k)].astype(f32)
+        normed = (part * scale * egain_ref[:, columns(k)]).astype(bf16)
+        of(zs, k)[...] = dot(place, normed).astype(bf16).reshape(zs.shape[1:3] + (widths[k],))
+        of(zr, k, z)[...] = of(zs, k, z)[...]
+
+    def wide_0():
+        part = x_ref[:, wide].astype(f32)
+        tk[0] = (part * scale * egain_ref[:, wide]).astype(bf16).reshape(tk.shape[1:])
+        remote(tk.at[0], tk.at[1], q_send.at[0], q_recv.at[0], tp=up1).start()
+        remote(tk.at[0], tk.at[2], q_send.at[0], q_recv.at[1], tp=down1).start()
+        remote(lg.at[0], lg.at[1], q_send.at[1], q_recv.at[4], tp=up1).start()
+        remote(lg.at[0], lg.at[2], q_send.at[1], q_recv.at[5], tp=down1).start()
+
+    def wide_1():
+        for i, to in ((0, up1), (1, down1)):
+            await_bytes(tk.at[1 + i], q_recv.at[i])
+            remote(tk.at[1 + i, i], tk.at[3, i], q_send.at[0], q_recv.at[2 + i], tp=to).start()
+        await_bytes(lg.at[1], q_recv.at[4])
+        remote(lg.at[1], lg.at[3], q_send.at[1], q_recv.at[6], tp=up1).start()
+
+    def wide_2():
+        for i in range(2):
+            await_bytes(tk.at[3, i], q_recv.at[2 + i])
+        for rel in range(Y):
+            put = place if rel == 0 else tables(owners[rel], logits_ref[...])[0]
+            block = dot(put, tk[rel].reshape(-1, wq)).astype(bf16)
+            zsq[:, rel] = block.reshape(Z, -1, wq)
+        z_peers(lambda d: remote(zsq.at[d], zrq.at[z], q_send.at[2], q_recv.at[7], ep_0=d).start())
+        zrq[z] = zsq[z]
+
+    def wide_3():
+        await_bytes(zrq.at[pl.ds(0, Z - 1)], q_recv.at[7])
+        for rel in range(Y):
+            block = dot(to_xc, zrq[:, rel].reshape(-1, wq)).astype(bf16)
+            xsq[:, rel] = block.reshape(XC, -1, wq)
+        xc_peers(
+            lambda j, a, b: remote(
+                xsq.at[j], arrq.at[:, xc], q_send.at[3], q_recv.at[8], ep_1=a, ep_2=b
+            ).start()
+        )
+        arrq[:, xc] = xsq[xc]
+
+    def wide_4():
+        await_bytes(arrq.at[:, pl.ds(0, XC - 1)], q_recv.at[8])
+        gathered = arrq[...].reshape(-1, wq)
+        for acc, w in ((gacc, gate_v), (uacc, up_v)):
+            acc[...] += dot_nt(gathered, w[:, wide])
+
+    def wide_5():
+        part = dot(hb[...], down_v[:, wide])
+        psq[...] = part.astype(bf16).reshape(psq.shape)
+        xc_peers(
+            lambda j, a, b: remote(
+                psq.at[:, j], xbq.at[xc], q_send.at[4], q_recv.at[9], ep_1=a, ep_2=b
+            ).start()
+        )
+        xbq[xc] = psq[:, xc]
+
+    def wide_6():
+        await_bytes(xbq.at[pl.ds(0, XC - 1)], q_recv.at[9])
+        for rel in range(Y):
+            block = dot(to_z, xbq[:, rel].reshape(-1, wq)).astype(bf16)
+            rzsq[:, rel] = block.reshape(Z, -1, wq)
+        z_peers(
+            lambda d: remote(rzsq.at[d], rzrq.at[z], q_send.at[5], q_recv.at[10], ep_0=d).start()
+        )
+        rzrq[z] = rzsq[z]
+
+    def weighed(table, results):
+        table = table.T
+        hi = table.astype(bf16)
+        low = (table - hi.astype(f32)).astype(bf16)
+        return dot(hi, results) + dot(low, results)
+
+    def wide_7():
+        await_bytes(rzrq.at[pl.ds(0, Z - 1)], q_recv.at[10])
+        await_bytes(lg.at[2], q_recv.at[5])
+        await_bytes(lg.at[3], q_recv.at[6])
+        for rel in range(Y):
+            table = tables(owners[rel], lg[rel][:TOP, :tokens])[1]
+            part = weighed(table, rzrq[:, rel].reshape(-1, wq))
+            uq[rel] = part.astype(bf16).reshape(uq.shape[1:])
+        for i, to in ((0, up1), (1, down1)):
+            remote(uq.at[3, i], t1.at[i], q_send.at[6], q_recv.at[11 + i], tp=to).start()
+
+    def wide_8():
+        for i, rel, to in ((0, 2, up1), (1, 1, down1)):
+            await_bytes(t1.at[i], q_recv.at[11 + i])
+            uq[rel, i] = (uq[rel, i].astype(f32) + t1[i].astype(f32)).astype(bf16)
+            remote(uq.at[rel], t2.at[i], q_send.at[7], q_recv.at[13 + i], tp=to).start()
+
+    def wide_9():
+        await_bytes(t2.at[0], q_recv.at[13])
+        await_bytes(t2.at[1], q_recv.at[14])
+        total = uq[0].astype(f32) + t2[0].astype(f32) + t2[1].astype(f32)
+        moe_ref[:, wide] = total.astype(bf16).reshape(tokens, wq)
+
+    lg[0] = jnp.zeros(lg.shape[1:], f32)
+    lg[0, :TOP, :tokens] = logits_ref[...]
 
     def z_go(k):
         z_peers(
             lambda d: remote(
-                zs.at[k, d], zr.at[k, z], z_send.at[k], z_recv.at[k], ep_0=d
+                of(zs, k, d), of(zr, k, z), z_send.at[k], z_recv.at[k], ep_0=d
             ).start()
         )
 
@@ -168,49 +296,51 @@
         if k == 0:
             pl.semaphore_wait(barrier, Z - 1 + XC - 1 + 2)
         z_go(k)
+        if k == 0:
+            wide_0()
 
     to_xc = regroup(XC, Z, 2)
     to_z = regroup(Z, XC, 2)
 
     def step_a(k):
-        await_bytes(zr.at[k, pl.ds(0, Z - 1)], z_recv.at[k])
-        block = dot(to_xc, zr[k].reshape(-1, W)).astype(bf16)
-        xs[k] = block.reshape(xs.shape[1:])
+        await_bytes(of(zr, k, pl.ds(0, Z - 1)), z_recv.at[k])
+        block = dot(to_xc, of(zr, k)[...].reshape(-1, widths[k])).astype(bf16)
+        of(xs, k)[...] = block.reshape(xs.shape[1:3] + (widths[k],))
         xc_peers(
             lambda j, a, b: remote(
-                xs.at[k, j], arr.at[k, 0, xc], x_send.at[k], x_recv.at[k], ep_1=a, ep_2=b
+                of(xs, k, j), of(arr, k, 0, xc), x_send.at[k], x_recv.at[k], ep_1=a, ep_2=b
             ).start()
         )
-        arr[k, 0, xc] = xs[k, xc]
+        of(arr, k, 0, xc)[...] = of(xs, k, xc)[...]
 
     def step_b(k):
-        await_bytes(arr.at[k, 0, pl.ds(0, XC - 1)], x_recv.at[k])
-        remote(arr.at[k, 0], arr.at[k, 1], y_send.at[k], y_recv.at[k, 0], tp=up1).start()
-        remote(arr.at[k, 0], arr.at[k, 2], y_send.at[k], y_recv.at[k, 1], tp=down1).start()
+        await_bytes(of(arr, k, 0, pl.ds(0, XC - 1)), x_recv.at[k])
+        remote(of(arr, k, 0), of(arr, k, 1), y_send.at[k], y_recv.at[k, 0], tp=up1).start()
+        remote(of(arr, k, 0), of(arr, k, 2), y_send.at[k], y_recv.at[k, 1], tp=down1).start()
 
     half = XC // 2
 
     def step_c(k):
-        await_bytes(arr.at[k, 1], y_recv.at[k, 0])
+        await_bytes(of(arr, k, 1), y_recv.at[k, 0])
         low = pl.ds(0, half)
         remote(
-            arr.at[k, 1, low], arr.at[k, 3, low], y_send.at[k], y_recv.at[k, 2], tp=up1
+            of(arr, k, 1, low), of(arr, k, 3, low), y_send.at[k], y_recv.at[k, 2], tp=up1
         ).start()
-        await_bytes(arr.at[k, 2], y_recv.at[k, 1])
+        await_bytes(of(arr, k, 2), y_recv.at[k, 1])
         high = pl.ds(half, half)
         remote(
-            arr.at[k, 2, high], arr.at[k, 3, high], y_send.at[k], y_recv.at[k, 3], tp=down1
+            of(arr, k, 2, high), of(arr, k, 3, high), y_send.at[k], y_recv.at[k, 3], tp=down1
         ).start()
 
     def step_d(k):
-        await_bytes(arr.at[k, 3, pl.ds(0, half)], y_recv.at[k, 2])
-        await_bytes(arr.at[k, 3, pl.ds(half, half)], y_recv.at[k, 3])
+        await_bytes(of(arr, k, 3, pl.ds(0, half)), y_recv.at[k, 2])
+        await_bytes(of(arr, k, 3, pl.ds(half, half)), y_recv.at[k, 3])
         if k == 0:
             weights[0].wait()
             weights[1].wait()
-        tokens = arr[k].reshape(-1, W)
+        tokens = of(arr, k)[...].reshape(-1, widths[k])
         for acc, w in ((gacc, gate_v), (uacc, up_v)):
-            part = dot_nt(tokens, w[:, k * W : (k + 1) * W])
+            part = dot_nt(tokens, w[:, columns(k)])
             if k == 0:
                 acc[...] = part
             elif k < NC - 1:
@@ -221,6 +351,8 @@
                 hb[...] = (jax.nn.silu(gate) * (acc[...] + part)).astype(bf16)
 
     def recurrence():
+        for copy in inputs[1:4]:
+            copy.wait()
         shut = jax.nn.sigmoid(-f_ref[...].astype(f32)) * margin_ref[...]
         tri = jnp.where(
             lax.broadcasted_iota(jnp.int32, (seq, seq), 0)
@@ -317,6 +449,7 @@
         remote(s5.at[c], s5.at[c], s_send.at[4], s_recv.at[4], ep_2=1 - c).start()
 
     def mix():
+        inputs[4].wait()
         await_bytes(s5.at[1 - c], s_recv.at[4])
         for h in range(heads):
             cols = slice(h * key, (h + 1) * key)
@@ -328,9 +461,9 @@
             gate = og_ref[:, cols].astype(f32)
             ha[:, cols] = (out * hgain_ref[:, cols] * jax.nn.silu(gate)).astype(bf16)
         weights[2].wait()
-        for k in range(NC):
-            at = slice(k * W, (k + 1) * W)
-            mp[:, :, :, at] = dot(ha[...], wo_v[:, at]).astype(bf16).reshape(mp.shape[:3] + (W,))
+        for at in [columns(k) for k in range(NC)] + [wide]:
+            part = dot(ha[...], wo_v[:, at]).astype(bf16)
+            mp[:, :, :, at] = part.reshape(mp.shape[:3] + (at.stop - at.start,))
 
     def mix_a():
         remote(mp.at[across, 0], m1.at[0], m_send.at[0], m_recv.at[0], tp=up1).start()
@@ -351,95 +484,117 @@
     def step_e(k):
         if k == 0:
             weights[3].wait()
-        part = dot(hb[...], down_v[:, k * W : (k + 1) * W])
-        ps[k] = part.astype(bf16).reshape(ps.shape[1:])
-        remote(ps.at[k, 3, 0], r1.at[k, 0], ra_send.at[k], r_recv.at[k, 0], tp=up1).start()
-        remote(ps.at[k, 3, 1], r1.at[k, 1], ra_send.at[k], r_recv.at[k, 1], tp=down1).start()
+        part = dot(hb[...], down_v[:, columns(k)])
+        of(ps, k)[...] = part.astype(bf16).reshape(ps.shape[1:4] + (widths[k],))
+        for i, to in ((0, up1), (1, down1)):
+            remote(of(ps, k, 3, i), of(r1, k, i), ra_send.at[k], r_recv.at[k, i], tp=to).start()
 
     def step_f(k):
         for i, rel, to in ((0, 2, up1), (1, 1, down1)):
-            await_bytes(r1.at[k, i], r_recv.at[k, i])
-            ps[k, rel, i] = (ps[k, rel, i].astype(f32) + r1[k, i].astype(f32)).astype(bf16)
-            remote(ps.at[k, rel], r2.at[k, i], rb_send.at[k], r_recv.at[k, 2 + i], tp=to).start()
+            await_bytes(of(r1, k, i), r_recv.at[k, i])
+            mine = of(ps, k, rel, i)
+            mine[...] = (mine[...].astype(f32) + of(r1, k, i)[...].astype(f32)).astype(bf16)
+            remote(
+                of(ps, k, rel), of(r2, k, i), rb_send.at[k], r_recv.at[k, 2 + i], tp=to
+            ).start()
 
     def step_g(k):
-        await_bytes(r2.at[k, 0], r_recv.at[k, 2])
-        await_bytes(r2.at[k, 1], r_recv.at[k, 3])
-        total = ps[k, 0].astype(f32) + r2[k, 0].astype(f32) + r2[k, 1].astype(f32)
-        rx[k] = total.astype(bf16).reshape(rx.shape[1:])
+        await_bytes(of(r2, k, 0), r_recv.at[k, 2])
+        await_bytes(of(r2, k, 1), r_recv.at[k, 3])
+        total = of(ps, k, 0)[...].astype(f32)
+        for i in range(2):
+            total = total + of(r2, k, i)[...].astype(f32)
+        of(rx, k)[...] = total.astype(bf16).reshape(rx.shape[1:3] + (widths[k],))
         xc_peers(
             lambda j, a, b: remote(
-                rx.at[k, j], xb.at[k, xc], rx_send.at[k], rx_recv.at[k], ep_1=a, ep_2=b
+                of(rx, k, j), of(xb, k, xc), rx_send.at[k], rx_recv.at[k], ep_1=a, ep_2=b
             ).start()
         )
-        xb[k, xc] = rx[k, xc]
+        of(xb, k, xc)[...] = of(rx, k, xc)[...]
 
     def step_h(k):
-        await_bytes(xb.at[k, pl.ds(0, XC - 1)], rx_recv.at[k])
-        block = dot(to_z, xb[k].reshape(-1, W)).astype(bf16)
-        rzs[k] = block.reshape(rzs.shape[1:])
+        await_bytes(of(xb, k, pl.ds(0, XC - 1)), rx_recv.at[k])
+        block = dot(to_z, of(xb, k)[...].reshape(-1, widths[k])).astype(bf16)
+        of(rzs, k)[...] = block.reshape(rzs.shape[1:3] + (widths[k],))
         z_peers(
             lambda d: remote(
-                rzs.at[k, d], rzr.at[k, z], rz_send.at[k], rz_recv.at[k], ep_0=d
+                of(rzs, k, d), of(rzr, k, z), rz_send.at[k], rz_recv.at[k], ep_0=d
             ).start()
         )
-        rzr[k, z] = rzs[k, z]
+        of(rzr, k, z)[...] = of(rzs, k, z)[...]
 
     comb = comb.T
     comb_hi = comb.astype(bf16)
     comb_lo = (comb - comb_hi.astype(f32)).astype(bf16)
 
     def step_i(k):
-        await_bytes(rzr.at[k, pl.ds(0, Z - 1)], rz_recv.at[k])
-        results = rzr[k].reshape(-1, W)
-        moe_ref[:, k * W : (k + 1) * W] = (dot(comb_hi, results) + dot(comb_lo, results)).astype(bf16)
+        await_bytes(of(rzr, k, pl.ds(0, Z - 1)), rz_recv.at[k])
+        results = of(rzr, k)[...].reshape(-1, widths[k])
+        moe_ref[:, columns(k)] = (dot(comb_hi, results) + dot(comb_lo, results)).astype(bf16)
 
     recurrence()
-    for t in range(NC + 3):
+    wide_1()
+    lag_b, lag_c, lag_d = OUT_LAGS
+    for t in range(NC + lag_d):
         if t < NC:
             step_a(t)
         if t == NC + 1:
             mix()
-        if 0 <= t - 1 < NC:
-            step_b(t - 1)
-        if 0 <= t - 2 < NC:
-            step_c(t - 2)
-        if t == NC + 1:
+        if 0 <= t - lag_b < NC:
+            step_b(t - lag_b)
+        if 0 <= t - lag_c < NC:
+            step_c(t - lag_c)
+        if t - lag_c == NC - 1:
             mix_a()
         if t == 0:
             state_2()
         if t == 1:
             state_3()
+            wide_2()
+        if t == NC + WIDE_AT[0]:
+            wide_3()
+        if t - lag_d == NC - 1:
+            wide_4()
         if t == NC:
             state_4()
-        if 0 <= t - 3 < NC:
-            step_d(t - 3)
+        if 0 <= t - lag_d < NC:
+            step_d(t - lag_d)
         if t == NC:
             state_5()
-    for t in range(NC + 4):
+    lag_f, lag_g, lag_h, lag_i = BACK_LAGS
+    for t in range(NC + lag_i):
         if t < NC:
             step_e(t)
-        if 0 <= t - 1 < NC:
-            step_f(t - 1)
-        if t == NC:
+        if t == 1:
+            wide_5()
+        if t == WIDE_AT[1]:
+            wide_6()
+        if t == NC + WIDE_AT[2]:
+            wide_7()
+        if 0 <= t - lag_f < NC:
+            step_f(t - lag_f)
+        if t - lag_f == NC - 1:
             mix_b()
-        if 0 <= t - 2 < NC:
-            step_g(t - 2)
-        if 0 <= t - 3 < NC:
-            step_h(t - 3)
-        if t == NC + 2:
+        if t == NC + WIDE_AT[3]:
+            wide_8()
+        if 0 <= t - lag_g < NC:
+            step_g(t - lag_g)
+        if 0 <= t - lag_h < NC:
+            step_h(t - lag_h)
+        if t - lag_i == NC - 1:
             mix_c()
-        if 0 <= t - 4 < NC:
-            step_i(t - 4)
+            wide_9()
+        if 0 <= t - lag_i < NC:
+            step_i(t - lag_i)
 
     for k in range(NC):
-        await_bytes(zs.at[k, pl.ds(0, Z - 1)], z_send.at[k])
-        await_bytes(xs.at[k, pl.ds(0, XC - 1)], x_send.at[k])
-        await_bytes(arr.at[k, pl.ds(0, 3)], y_send.at[k])
-        await_bytes(ps.at[k, 3], ra_send.at[k])
-        await_bytes(ps.at[k, pl.ds(1, 2)], rb_send.at[k])
-        await_bytes(rx.at[k, pl.ds(0, XC - 1)], rx_send.at[k])
-        await_bytes(rzs.at[k, pl.ds(0, Z - 1)], rz_send.at[k])
+        await_bytes(of(zs, k, pl.ds(0, Z - 1)), z_send.at[k])
+        await_bytes(of(xs, k, pl.ds(0, XC - 1)), x_send.at[k])
+        await_bytes(of(arr, k, pl.ds(0, 3)), y_send.at[k])
+        await_bytes(of(ps, k, 3), ra_send.at[k])
+        await_bytes(of(ps, k, pl.ds(1, 2)), rb_send.at[k])
+        await_bytes(of(rx, k, pl.ds(0, XC - 1)), rx_send.at[k])
+        await_bytes(of(rzs, k, pl.ds(0, Z - 1)), rz_send.at[k])
     await_bytes(mp.at[0], m_send.at[0])
     await_bytes(mp.at[pl.ds(0, 2)], m_send.at[1])
     await_bytes(s1.at[0], s_send.at[0])
@@ -447,6 +602,14 @@
     await_bytes(s3.at[pl.ds(0, Z - 1)], s_send.at[2])
     await_bytes(s4.at[pl.ds(0, X - 1)], s_send.at[3])
     await_bytes(s5.at[0], s_send.at[4])
+    await_bytes(tk.at[pl.ds(0, 3)], q_send.at[0])
+    await_bytes(lg.at[pl.ds(0, 3)], q_send.at[1])
+    await_bytes(zsq.at[pl.ds(0, Z - 1)], q_send.at[2])
+    await_bytes(xsq.at[pl.ds(0, XC - 1)], q_send.at[3])
+    await_bytes(psq.at[:, pl.ds(0, XC - 1)], q_send.at[4])
+    await_bytes(rzsq.at[pl.ds(0, Z - 1)], q_send.at[5])
+    await_bytes(uq.at[3], q_send.at[6])
+    await_bytes(uq.at[pl.ds(1, 2)], q_send.at[7])
 
 
 def slot_tables(chosen, logits, experts):
@@ -494,7 +657,8 @@
     expert_up_matrix,
     expert_down_matrix,
 ):
-    Z, X, C, Y, NC = sizes
+    Z, X, C, Y, shares = sizes
+    NC = len(shares)
     XC = X * C
     experts = Z * XC
     tokens, D = second_micro_input.shape
@@ -502,7 +666,9 @@
     heads = surge_log_decay.shape[0]
     key = width // heads
     F = expert_gate_matrix.shape[2]
-    W = D // NC
+    widths = tuple(D * share // (sum(shares) + WIDE) for share in shares)
+    wq = D - sum(widths)
+    W = max(widths)
     slots = 2 * experts
     V = pltpu.VMEM
     DMA = pltpu.SemaphoreType.DMA
@@ -536,6 +702,27 @@
         V((seq, width), f32),
         V((heads, seq, key), bf16),
         V((seq, width), bf16),
+        V((Y, 2, tokens // 2, wq), bf16),
+        V((Z, Y, 2 * XC, wq), bf16),
+        V((Z, Y, 2 * XC, wq), bf16),
+        V((XC, Y, 2 * Z, wq), bf16),
+        V((Y, XC, 2 * Z, wq), bf16),
+        V((Y, XC, 2 * Z, wq), bf16),
+        V((XC, Y, 2 * Z, wq), bf16),
+        V((Z, Y, 2 * XC, wq), bf16),
+        V((Z, Y, 2 * XC, wq), bf16),
+        V((Y, 2, tokens // 2, wq), bf16),
+        V((2, tokens // 2, wq), bf16),
+        V((2, 2, tokens // 2, wq), bf16),
+        V((Y, 8, 128), f32),
+        DMA((8,)),
+        DMA((15,)),
+        V((seq, width), bf16),
+        V((seq, width), bf16),
+        V((seq, width), bf16),
+        V((seq, width), bf16),
+        V((tokens, D), bf16),
+        DMA((5,)),
         DMA((4,)),
         DMA((NC,)),
         DMA((NC,)),
@@ -559,9 +746,9 @@
     hbm = pl.BlockSpec(memory_space=pl.ANY)
     out = jax.ShapeDtypeStruct((tokens, D), bf16)
     results = pl.pallas_call(
-        functools.partial(kernel, sizes),
+        functools.partial(kernel, sizes[:4] + (widths,)),
         out_shape=(jax.ShapeDtypeStruct((seq // Y, D), bf16), out),
-        in_specs=[vmem] * 11 + [hbm] * 4,
+        in_specs=[hbm] * 4 + [vmem] * 3 + [hbm] + [vmem] * 3 + [hbm] * 4,
         out_specs=(vmem, vmem),
         scratch_shapes=scratch,
         compiler_params=pltpu.CompilerParams(

time: 117 us -> 110 us (0.940)
  Pallas kernels: 117 us -> 109 us
    pallas_call x1, Pallas kernels: 115 us -> 107 us  [per_device(): pl.pallas_call(functools.partial(kernel, sizes[:4] + (widths,)), out_shap...]
where the time goes in v3:
time: 110 us
  Pallas kernels  109 us (99%)
    pallas_call x1, Pallas kernels, per_device(): pl.pallas_call(functools.partial(kernel, sizes[:4] + (widths,)), out_shap...  107 us

profile of v3, /device:TPU:1, one launch (start us, length us, event | category | flops | bytes accessed | tf_op | source)
XLA Modules:
  0.0 109.8 jit_solution(8697146610384494339)
XLA Ops:
  0.6 107.4 %shard_map.158 = (bf16[32,4096]{1,0:T(8,128)(2,1)}, bf16[32,4096]{1,0:T(8,128)(2,1)}) custom-call(bf16[128,256]{1,0:T(8,128)(2,1)} %q_hbm.1, bf16[128,256]{1,0:T(8,128)(2,1)} %f_hbm.1, bf16[128,256]{1,0:T(8,128)(2,1)} %v_hbm.1, bf16[128,256]{1,0:T(8,128)(2,1)} %og_hbm.1, f32[1,256]{1,0:T(1,128)} %bitcast.16, f32[2,128]{1,0:T(2,128)} %surge_ref.1, ...), custom_call_target="tpu_custom_call" | custom-call | tf_op jit(solution)/shard_map/pallas_call | solution.py:748
  108.0 1.8 %shard_map.159 = (bf16[32,4096]{1,0:T(8,128)(2,1)}, bf16[32,4096]{1,0:T(8,128)(2,1)}) custom-call(bf16[32,4096]{1,0:T(8,128)(2,1)} %get-tuple-element.4.mixed_in, bf16[32,4096]{1,0:T(8,128)(2,1)} %get-tuple-element.5.moe_in), custom_call_target="tpu_custom_call" | custom-call | tf_op jit(solution)/shard_map/pallas_call | solution.py:774
